TPU v7x, 128 devices: a whole 4x4x4 slice. The times are simulated.
128 devices in a mesh: ep: 32 (over z, y, core), tp: 4 (over x).
Axes of the slice: x: 4, y: 4, z: 4, core: 2. Of those that a mesh axis runs over, the one named last changes fastest.
Arguments:
- queries: bfloat16 [65536, 1024], P('ep', 'tp'), may hold values from -6 to 6
- keys_values: bfloat16 [65536, 512], P('ep', 'tp'), may hold values from -6 to 6
- sink_logits: float32 [16], replicated, may hold values from 4 to 8
- out_weight: bfloat16 [1024, 2048], replicated, may hold values from -4 to 4
- expert_tokens: bfloat16 [32768, 2048], P(('ep', 'tp')), may hold values from -6 to 6
- norm_gain: float32 [2048], replicated, may hold values from 0.1 to 1.9
- routes: int32 [32768, 2], P(('ep', 'tp')), may hold values from 0 to 31, all different within a row; in each aligned block of 256 rows (0 to 255, 256 to 511, ...) at most 24 rows name the same one
- route_weights: float32 [32768, 2], P(('ep', 'tp')), may hold values from 0.1 to 1
- gate_weight: bfloat16 [32, 2048, 1024], P('ep', None, 'tp'), may hold values from -0.125 to 0.125
- up_weight: bfloat16 [32, 2048, 1024], P('ep', None, 'tp'), may hold values from -0.125 to 0.125
- down_weight: bfloat16 [32, 1024, 2048], P('ep', 'tp'), may hold values from -0.1875 to 0.1875
Outputs:
- mixer_out: bfloat16 [65536, 2048], P(('ep', 'tp'))
- expert_out: bfloat16 [32768, 2048], P(('ep', 'tp'))
Inputs may be any that keep to these rules, and one draw needn't show every extreme that they name: `routes`: each row names 2 different experts. In each aligned block of 256 rows, no expert is named by more than 24 rows, and in some block an expert is named by exactly 24 rows.
All inputs are finite; a program needn't handle non-finite values.
Results may differ from a plain program's by a relative error of at most 0.012.
Values may be sent and summed in bfloat16 or wider, within the bound.
A program may use at most 128 MiB of HBM per device.

v0:
```python
import jax
import jax.numpy as jnp
from jax import lax
from jax.sharding import Mesh
from jax.sharding import PartitionSpec as P

HEAD_DIM = 64
WINDOW = 128
TOPK = 2
EP = ("ep_0", "ep_1", "ep_2")
EP_TP = ("ep_0", "ep_1", "ep_2", "tp")


NEG_FILL = -1e30


def padded_2(cells, sides, width):
    for axis, dim in sides:
        count = lax.axis_size(axis)
        ends = count - 1
        head = lax.slice_in_dim(cells, 0, width, axis=dim)
        tail = lax.slice_in_dim(cells, cells.shape[dim] - width, cells.shape[dim], axis=dim)
        cells = jnp.concatenate(
            [
                lax.ppermute(tail, axis, [(i, (i + 1) % count) for i in range(ends)]),
                cells,
                lax.ppermute(head, axis, [((i + 1) % count, i) for i in range(ends)]),
            ],
            axis=dim,
        )
    return cells


def rows_first(arrays, axis, dims):
    turned = [jnp.moveaxis(a, dim, 0) for a, dim in zip(arrays, dims)]
    both = jnp.concatenate([t.reshape(len(t), -1) for t in turned], axis=1)
    filled, at, done = (lax.all_gather(both, axis, axis=0, tiled=True), 0, [])
    for t, dim in zip(turned, dims):
        piece = filled[:, at : at + t[0].size].reshape(-1, *t.shape[1:])
        done.append(jnp.moveaxis(piece, 0, dim))
        at += t[0].size
    return tuple(done)


def split_up(x, dim, length):
    dims = x.shape
    tiles = x.reshape(*dims[:dim], length, dims[dim] // length, *dims[dim + 1 :])
    return jnp.moveaxis(tiles, dim, 0)


def in_order(tiles, dim):
    dims = list(tiles.shape[1:])
    dims[dim] *= tiles.shape[0]
    return jnp.moveaxis(tiles, 0, dim).reshape(dims)


def exchange_in_order(tiles, axes, sequence):
    inside = tiles.shape[1:]
    filled = tiles.reshape(*(lax.axis_size(a) for a in axes), *inside)
    for k in sequence:
        filled = lax.all_to_all(filled, axes[k], k, k, tiled=True)
    return filled.reshape(-1, *inside)


def two_step_exchange(x, groups, sequence, split_dim, concat_dim):
    length = lax.axis_size(groups[0]) * lax.axis_size(groups[1])
    tiles = split_up(x, split_dim, length)
    return in_order(exchange_in_order(tiles, groups, sequence), concat_dim)


def widen_rows(token_rows, gate_local, up_local):
    gate_value = jnp.einsum(
        "etcd,df->etcf", token_rows, gate_local, preferred_element_type=jnp.float32
    )
    up_value = jnp.einsum("etcd,df->etcf", token_rows, up_local, preferred_element_type=jnp.float32)
    return (jax.nn.silu(gate_value) * up_value).astype(jnp.bfloat16)


def attend(queries, keys_values, sink_logits):
    row_count = queries.shape[0]
    kv_local = keys_values.shape[1] // (2 * HEAD_DIM)
    group_size = queries.shape[1] // (kv_local * HEAD_DIM)
    block_rows = min(512, row_count)
    key_span = block_rows + 2 * WINDOW
    padded = padded_2(keys_values, ((EP, 0),), WINDOW)
    offset = lax.axis_index(EP) * row_count
    seq_total = row_count * lax.axis_size(EP)
    head_first = lax.axis_index("tp") * (kv_local * group_size)
    sink_local = lax.dynamic_slice_in_dim(
        sink_logits, head_first, kv_local * group_size, 0
    ).reshape(kv_local, group_size, 1, 1)
    score_scale = HEAD_DIM ** (-0.5)

    def one_block(block_index):
        first_row = block_index * block_rows
        query_block = lax.dynamic_slice_in_dim(queries, first_row, block_rows, 0).reshape(
            block_rows, kv_local, group_size, HEAD_DIM
        )
        pair_block = lax.dynamic_slice_in_dim(padded, first_row, key_span, 0).reshape(
            key_span, kv_local, 2, HEAD_DIM
        )
        scores = (
            jnp.einsum(
                "qhgd,khd->hgqk",
                query_block,
                pair_block[:, :, 0],
                preferred_element_type=jnp.float32,
            )
            * score_scale
        )
        query_pos = offset + first_row + jnp.arange(block_rows, dtype=jnp.int32)
        key_pos = offset + first_row - WINDOW + jnp.arange(key_span, dtype=jnp.int32)
        allowed = (
            (jnp.abs(query_pos[:, None] - key_pos[None, :]) <= WINDOW)
            & (key_pos >= 0)[None, :]
            & (key_pos < seq_total)[None, :]
        )
        scores = jnp.where(allowed, scores, NEG_FILL)
        top_score = jnp.maximum(jnp.max(scores, -1, keepdims=True), sink_local)
        exp_scores = jnp.exp(scores - top_score)
        denominator = jnp.sum(exp_scores, -1, keepdims=True) + jnp.exp(sink_local - top_score)
        attn_weights = (exp_scores / denominator).astype(jnp.bfloat16)
        head_values = jnp.einsum(
            "hgqk,khd->qhgd", attn_weights, pair_block[:, :, 1], preferred_element_type=jnp.float32
        )
        return head_values.astype(jnp.bfloat16).reshape(
            block_rows, kv_local * group_size * HEAD_DIM
        )

    blocks = lax.map(one_block, jnp.arange(row_count // block_rows, dtype=jnp.int32))
    return blocks.reshape(row_count, kv_local * group_size * HEAD_DIM)


def body(
    queries,
    keys_values,
    sink_logits,
    out_weight,
    expert_tokens,
    norm_gain,
    routes,
    route_weights,
    gate_weight,
    up_weight,
    down_weight,
):
    tp_count = lax.axis_size("tp")
    ep_count = lax.axis_size(EP)
    attended = attend(queries, keys_values, sink_logits)
    token_rows = lax.all_to_all(attended, "tp", split_axis=0, concat_axis=1, tiled=True)
    mixer_out = jnp.dot(token_rows, out_weight, preferred_element_type=jnp.float32).astype(
        jnp.bfloat16
    )
    row_count = expert_tokens.shape[0]
    model_width = expert_tokens.shape[1]
    capacity = 3 * row_count * TOPK // (2 * ep_count)
    rows_float = expert_tokens.astype(jnp.float32)
    centred = rows_float - jnp.mean(rows_float, -1, keepdims=True)
    normed = (
        centred * lax.rsqrt(jnp.mean(centred * centred, -1, keepdims=True) + 1e-06) * norm_gain
    ).astype(jnp.bfloat16)
    flat_routes = routes.reshape(-1)
    one_hot = (flat_routes[:, None] == jnp.arange(ep_count, dtype=jnp.int32)[None, :]).astype(
        jnp.int32
    )
    slot_rank = jnp.sum((jnp.cumsum(one_hot, 0) - 1) * one_hot, 1)
    slot_index = flat_routes * capacity + slot_rank
    copy_token = jnp.arange(row_count * TOPK, dtype=jnp.int32) // TOPK
    slot_token = (
        jnp.full((ep_count * capacity,), row_count, jnp.int32).at[slot_index].set(copy_token)
    )
    outgoing = jnp.take(normed, slot_token, axis=0, mode="fill", fill_value=0).reshape(
        ep_count, capacity, model_width
    )
    gate_local = gate_weight[0]
    up_local = up_weight[0]
    down_local = down_weight[0]
    gate_whole, up_whole, down_whole = rows_first(
        (gate_local, up_local, down_local), "tp", (1, 1, 0)
    )
    arrived = two_step_exchange(outgoing, (("ep_0", "ep_1"), "ep_2"), (1, 0), 0, 0)
    hidden = widen_rows(arrived[:, None], gate_whole, up_whole)
    block_width = down_local.shape[0]
    hidden_blocks = hidden.reshape(ep_count * capacity, tp_count, block_width)
    down_blocks = down_whole.reshape(tp_count, block_width, model_width)
    partial_value = jnp.einsum(
        "rqf,qfd->qrd", hidden_blocks, down_blocks, preferred_element_type=jnp.float32
    ).astype(jnp.bfloat16)
    expert_rows = jnp.sum(partial_value.astype(jnp.float32), 0).astype(jnp.bfloat16)
    returned = lax.all_to_all(
        expert_rows.reshape(ep_count, capacity, model_width),
        EP,
        split_axis=0,
        concat_axis=0,
        tiled=True,
    )
    per_copy = jnp.take(returned.reshape(ep_count * capacity, model_width), slot_index, axis=0)
    weighted = (
        per_copy.astype(jnp.float32).reshape(row_count, TOPK, model_width)
        * route_weights[:, :, None]
    )
    expert_out = jnp.sum(weighted, 1).astype(jnp.bfloat16)
    return (mixer_out, expert_out)


def solution(mesh):
    finer = Mesh(mesh.devices.reshape(4, 4, 2, mesh.shape["tp"]), ("ep_0", "ep_1", "ep_2", "tp"))
    in_specs = (
        P(EP, "tp"),
        P(EP, "tp"),
        P(),
        P(),
        P(EP_TP, None),
        P(),
        P(EP_TP, None),
        P(EP_TP, None),
        P(EP, None, "tp"),
        P(EP, None, "tp"),
        P(EP, "tp", None),
    )
    out_specs = (P(EP_TP, None), P(EP_TP, None))
    return jax.shard_map(body, mesh=finer, in_specs=in_specs, out_specs=out_specs, check_vma=False)
```

profile of v0, /device:TPU:0, one launch (start us, length us, event | category | flops | bytes accessed | tf_op | source)
XLA Modules:
  0.0 237.7 jit_solution(1574381252939616928)
XLA Ops:
  7.2 1.6 copy.66
  8.8 1.5 copy.67
  10.3 1.8 pad_maximum_fusion
  12.2 0.7 copy-done.6
  13.2 1.2 reduce-window.6
  14.4 0.2 slice_reduce_fusion
  15.1 2.4 %scatter_custom_fusion = s32[768]{0:T(1024)S(1)} fusion(s32[512]{0:T(512)S(1)} %bitcast.127, s32[512]{0:T(512)S(1)} %add_select_fusion, s32[]{:T(128)} %constant.156.clone.1), kind=kCustom, calls=%fused_computation.69 | custom fusion | bytes 3076 | tf_op jit(solution)/shard_map/scatter | solution.py:170
  17.7 0.2 convert_reduce_fusion.1
  18.0 0.4 fusion.18
  18.4 0.4 fusion.20
  18.8 4.3 %gather_fusion = bf16[768,2048]{1,0:T(8,128)(2,1)} fusion(bf16[256,2048]{1,0:T(8,128)(2,1)S(1)} %fusion.20, s32[1024]{0:T(1024)S(1)} %pad_clamp_fusion.1), kind=kCustom, calls=%fused_computation | custom fusion | bytes 6294528 | tf_op jit(solution)/shard_map/jit(_take)/gather | solution.py:172
  23.1 2.6 %copy_select_fusion = bf16[16,2,1,24,2048]{4,3,0,2,1:T(8,128)(2,1)S(1)} fusion(bf16[16,2,1,24,2048]{4,3,1,0,2:T(8,128)(2,1)} %bitcast.115, pred[16,2,24]{2,0,1:T(8,128)(4,1)S(1)} %copy.63), kind=kLoop, calls=%fused_computation.36 | loop fusion | flops 1572864 | bytes 6292224 | tf_op jit(solution)/shard_map/jit(_take)/select_n | solution.py:172
  25.8 6.3 %all_to_all.31 = bf16[16,2,1,24,2048]{4,3,0,2,1:T(8,128)(2,1)S(1)} all-to-all(bf16[16,2,1,24,2048]{4,3,0,2,1:T(8,128)(2,1)S(1)} %copy_select_fusion), channel_id=1, replica_groups=mesh['ep_0'=4,'ep_1'=4,'ep_2'=2,'tp'=4] {'ep_2'}, dimensions={1} | all-to-all | bytes 6291456 | tf_op jit(solution)/shard_map/all_to_all | solution.py:61
  32.0 2.1 copy.65
  34.1 8.4 %all-to-all-start.2 = ((bf16[16,2,1,24,2048]{4,3,1,2,0:T(8,128)(2,1)}), bf16[16,2,1,24,2048]{4,3,1,2,0:T(8,128)(2,1)}, u32[]{:S(2)}, u32[]{:S(2)}) async-start(bf16[16,2,1,24,2048]{4,3,1,2,0:T(8,128)(2,1)} %copy.65), calls=%async_computation.2 | async-start | bytes 6291456 | tf_op jit(solution)/shard_map/all_to_all | solution.py:61
  42.5 0.2 copy.53
  42.8 1.8 collective-permute-start
  44.5 1.3 collective-permute-start.1
  45.9 3.3 %collective-permute-done.1 = bf16[128,128]{0,1:T(8,128)(2,1)S(1)} collective-permute-done((bf16[128,128]{0,1:T(8,128)(2,1)S(1)}, bf16[128,128]{0,1:T(8,128)(2,1)S(1)}, u32[]{:S(2)}, u32[]{:S(2)}) %collective-permute-start.1) | collective-permute-done | bytes 32800 | tf_op jit(solution)/shard_map/ppermute | solution.py:27
  49.4 34.5 %while.12 = (s32[]{:T(128)}, bf16[4,512,256]{1,2,0:T(8,128)(2,1)}, s32[4]{0:T(128)S(1)}, bf16[2304,128]{0,1:T(8,128)(2,1)S(1)}, s32[]{:T(128)}, /*index=5*/bf16[...) while((s32[]{:T(128)}, bf16[4,512,256]{1,2,0:T(8,128)(2,1)}, ...), condition=%wide.region_3.4_spmd, body=%wide.region_0.3_spmd.sunk | while | flops 423632384 | bytes 23230236 | solution.py:130
  49.4 0.6 dynamic_slice.31
  50.7 0.8 fusion.47
  51.5 1.0 constant_dynamic-slice_fusion.4
  52.6 1.2 fusion.48
  53.9 1.4 fusion.49
  55.3 1.9 fusion.50
  57.3 0.7 constant_dynamic-update-slice_fusion.2
  58.0 0.6 dynamic_slice.31
  59.3 0.8 fusion.47
  60.1 1.0 constant_dynamic-slice_fusion.4
  61.2 1.2 fusion.48
  62.5 1.4 fusion.49
  64.0 1.9 fusion.50
  65.9 0.7 constant_dynamic-update-slice_fusion.2
  66.6 0.6 dynamic_slice.31
  67.9 0.8 fusion.47
  68.7 1.0 constant_dynamic-slice_fusion.4
  69.9 1.2 fusion.48
  71.1 1.4 fusion.49
  72.6 1.9 fusion.50
  74.5 0.7 constant_dynamic-update-slice_fusion.2
  75.2 0.6 dynamic_slice.31
  76.5 0.8 fusion.47
  77.4 1.0 constant_dynamic-slice_fusion.4
  78.5 1.2 fusion.48
  79.8 1.4 fusion.49
  81.2 1.9 fusion.50
  83.1 0.7 constant_dynamic-update-slice_fusion.2
  83.9 7.8 %all-to-all-done.2 = bf16[16,2,1,24,2048]{4,3,1,2,0:T(8,128)(2,1)} async-done(((bf16[16,2,1,24,2048]{4,3,1,2,0:T(8,128)(2,1)}), bf16[16,2,1,24,2048]{4,3,1,2,0:T(8,128)(2,1)}, u32[]{:S(2)}, u32[]{:S(2)}) %all-to-all-start.2) | async-done | bytes 3145760 | tf_op jit(solution)/shard_map/all_to_all | solution.py:61
  91.7 4.4 %all-to-all-start = ((bf16[4,512,256]{1,2,0:T(8,128)(2,1)}), bf16[4,512,256]{1,2,0:T(8,128)(2,1)}, u32[]{:S(2)}, u32[]{:S(2)}) async-start(bf16[4,512,256]{1,2,0:T(8,128)(2,1)} %get-tuple-element.91), calls=%async_computation | async-start | bytes 2097152 | tf_op jit(solution)/shard_map/all_to_all | solution.py:150
  96.2 46.6 %all-gather.2.cloned.1.call-done = bf16[1024,6144]{1,0:T(8,128)(2,1)} async-done(((bf16[256,6144]{1,0:T(8,128)(2,1)}), bf16[1024,6144]{1,0:T(8,128)(2,1)}) %all-gather.2.cloned.1.call-update) | async-done | bytes 12582928 | tf_op jit(solution)/shard_map/all_gather | solution.py:37
  142.8 6.4 %fusion.14 = f32[32,24,1024]{2,1,0:T(8,128)S(1)} fusion(bf16[32,24,2048]{2,1,0:T(8,128)(2,1)} %bitcast.21, bf16[1024,6144]{1,0:T(8,128)(2,1)} %all-gather.2.cloned.1.call-done), kind=kOutput, calls=%fused_computation.30 | convolution fusion | flops 3221225472 | bytes 10485760 | tf_op jit(solution)/shard_map/etcd,df->etcf/dot_general | solution.py:75
  149.1 0.4 copy-done.3
  149.5 5.7 %multiply_convert_fusion = bf16[32,24,1024]{2,1,0:T(8,128)(2,1)S(1)} fusion(f32[32,24,1024]{2,1,0:T(8,128)S(1)} %fusion.14, bf16[32,24,2048]{2,1,0:T(8,128)(2,1)} %bitcast.21, bf16[1024,6144]{1,0:T(8,128)(2,1)S(1)} %copy-done.3), kind=kOutput, calls=%fused_computation.37 | convolution fusion | flops 3225944064 | bytes 12058624 | tf_op jit(solution)/shard_map/etcd,df->etcf/dot_general | solution.py:72
  155.3 1.2 reshape.296
  156.5 2.2 slice-done
  158.6 6.4 %convert_reduce_fusion = bf16[768,2048]{1,0:T(8,128)(2,1)} fusion(bf16[4,256,2048]{2,1,0:T(8,128)(2,1)S(1)} %bitcast.119, bf16[768,4,256]{2,1,0:T(4,128)(2,1)S(1)} %reshape.296), kind=kOutput, calls=%fused_computation.28 | convolution fusion | flops 3232235520 | bytes 8912896 | tf_op jit(solution)/shard_map/rqf,qfd->qrd/dot_general | solution.py:186
  165.0 8.2 %all-to-all-start.3 = ((bf16[32,24,2048]{2,1,0:T(8,128)(2,1)}), bf16[32,24,2048]{2,1,0:T(8,128)(2,1)S(1)}, u32[]{:S(2)}, u32[]{:S(2)}) async-start(bf16[32,24,2048]{2,1,0:T(8,128)(2,1)} %bitcast.122), calls=%async_computation.3 | async-start | bytes 6291456 | tf_op jit(solution)/shard_map/all_to_all | solution.py:190
  173.5 0.2 copy.61
  173.9 6.2 %convolution_convert_fusion = bf16[512,2048]{1,0:T(8,128)(2,1)} fusion(bf16[512,1024]{0,1:T(8,128)(2,1)} %bitcast.16, bf16[1024,2048]{1,0:T(8,128)(2,1)} %param.16), kind=kOutput, calls=%fused_computation.38 | convolution fusion | flops 2148532224 | bytes 7340032 | tf_op jit(solution)/shard_map/dot_general | solution.py:151
  180.1 35.0 %all-to-all-done.3 = bf16[32,24,2048]{2,1,0:T(8,128)(2,1)S(1)} async-done(((bf16[32,24,2048]{2,1,0:T(8,128)(2,1)}), bf16[32,24,2048]{2,1,0:T(8,128)(2,1)S(1)}, u32[]{:S(2)}, u32[]{:S(2)}) %all-to-all-start.3) | async-done | bytes 3145760 | tf_op jit(solution)/shard_map/all_to_all | solution.py:190
  215.1 3.3 %gather_fusion.1 = bf16[512,2048]{1,0:T(8,128)(2,1)} fusion(bf16[768,2048]{1,0:T(8,128)(2,1)S(1)} %bitcast.113, s32[1024]{0:T(1024)S(1)} %pad_clamp_fusion), kind=kCustom, calls=%fused_computation.1 | custom fusion | bytes 4196352 | tf_op jit(solution)/shard_map/jit(_take)/gather | solution.py:197
  218.4 3.2 %gather.15 = bf16[256,2,2048]{2,1,0:T(2,128)(2,1)S(1)} reshape(bf16[512,2048]{1,0:T(8,128)(2,1)} %gather_fusion.1) | data formatting | bytes 4194304 | tf_op jit(solution)/shard_map/jit(_take)/gather | solution.py:197
  221.6 9.2 %multiply_reduce_fusion = bf16[256,2048]{1,0:T(8,128)(2,1)} fusion(bf16[256,2,2048]{2,1,0:T(2,128)(2,1)S(1)} %gather.15, pred[256,2]{1,0:T(8,128)(4,1)S(1)} %copy.61, f32[256,2]{1,0:T(8,128)S(1)} %copy.69), kind=kLoop, calls=%fused_computation.33 | loop fusion | flops 3670016 | bytes 3148288 | tf_op jit(solution)/shard_map/reduce_sum | solution.py:202
  (78 shorter events, 2.9 us)
Async XLA Ops:
  7.2 38.7 %copy-start = (f32[16]{0:T(128)S(1)}, f32[16]{0:T(128)}, u32[]{:S(2)}) copy-start(f32[16]{0:T(128)} %param.15) | copy-start | bytes 196
  7.2 3.1 %copy-start.4 = (bf16[1,256,2048]{2,1,0:T(8,128)(2,1)S(1)}, bf16[1,256,2048]{2,1,0:T(8,128)(2,1)}, u32[]{:S(2)}) copy-start(bf16[1,256,2048]{2,1,0:T(8,128)(2,1)} %param.23) | copy-start | bytes 3145732
  7.2 135.6 %all-gather.2.cloned.1.call-start = ((), (), s32[]{:S(2)}) async-start(), calls=%async_computation.4 | async-start | bytes 15728640 | tf_op jit(solution)/shard_map/all_gather | solution.py:37
  12.1 0.7 copy-start.6
  12.1 5.6 %copy-start.2 = (bf16[256,2048]{1,0:T(8,128)(2,1)S(1)}, bf16[256,2048]{1,0:T(8,128)(2,1)}, u32[]{:S(2)}) copy-start(bf16[256,2048]{1,0:T(8,128)(2,1)} %param.17) | copy-start | bytes 3145732
  12.1 6.3 %copy-start.7 = (f32[2048]{0:T(1024)S(1)}, f32[2048]{0:T(1024)}, u32[]{:S(2)}) copy-start(f32[2048]{0:T(1024)} %param.18) | copy-start | bytes 24580
  34.1 8.4 %copy-start.5 = (bf16[2048,128]{1,0:T(8,128)(2,1)S(1)}, bf16[2048,128]{1,0:T(8,128)(2,1)}, u32[]{:S(2)}) copy-start(bf16[2048,128]{1,0:T(8,128)(2,1)} %param.14) | copy-start | bytes 1572868
  34.1 57.6 %all-to-all-start.2 = ((bf16[16,2,1,24,2048]{4,3,1,2,0:T(8,128)(2,1)}), bf16[16,2,1,24,2048]{4,3,1,2,0:T(8,128)(2,1)}, u32[]{:S(2)}, u32[]{:S(2)}) async-start(bf16[16,2,1,24,2048]{4,3,1,2,0:T(8,128)(2,1)} %copy.65), calls=%async_computation.2 | async-start | bytes 6291456 | tf_op jit(solution)/shard_map/all_to_all | solution.py:61
  42.8 3.2 %collective-permute-start = (bf16[128,128]{0,1:T(8,128)(2,1)S(1)}, bf16[128,128]{0,1:T(8,128)(2,1)S(1)}, u32[]{:S(2)}, u32[]{:S(2)}) collective-permute-start(bf16[128,128]{0,1:T(8,128)(2,1)S(1)} %get-tuple-element.138), channel_id=1, source_target_pairs={{0,4},{4,8},{8,12},{12,16},{16,20},{20,24},{24,28},{28,32},{32,36}... | collective-permute-start | bytes 98312 | tf_op jit(solution)/shard_map/ppermute | solution.py:25
  44.5 4.7 %collective-permute-start.1 = (bf16[128,128]{0,1:T(8,128)(2,1)S(1)}, bf16[128,128]{0,1:T(8,128)(2,1)S(1)}, u32[]{:S(2)}, u32[]{:S(2)}) collective-permute-start(bf16[128,128]{0,1:T(8,128)(2,1)S(1)} %get-tuple-element.139), channel_id=1, source_target_pairs={{4,0},{8,4},{12,8},{16,12},{20,16},{24,20},{28,24},{32,28},{36,32}... | collective-permute-start | bytes 98312 | tf_op jit(solution)/shard_map/ppermute | solution.py:27
  91.7 73.3 %all-to-all-start = ((bf16[4,512,256]{1,2,0:T(8,128)(2,1)}), bf16[4,512,256]{1,2,0:T(8,128)(2,1)}, u32[]{:S(2)}, u32[]{:S(2)}) async-start(bf16[4,512,256]{1,2,0:T(8,128)(2,1)} %get-tuple-element.91), calls=%async_computation | async-start | bytes 2097152 | tf_op jit(solution)/shard_map/all_to_all | solution.py:150
  142.8 6.7 %copy-start.3 = (bf16[1024,6144]{1,0:T(8,128)(2,1)S(1)}, bf16[1024,6144]{1,0:T(8,128)(2,1)}, u32[]{:S(2)}) copy-start(bf16[1024,6144]{1,0:T(8,128)(2,1)} %all-gather.2.cloned.1.call-done) | copy-start | bytes 37748740
  156.5 2.2 slice-start
  165.0 8.7 %copy-start.8 = (f32[256,2]{0,1:T(2,128)S(1)}, f32[256,2]{0,1:T(2,128)}, u32[]{:S(2)}) copy-start(f32[256,2]{0,1:T(2,128)} %param.20) | copy-start | bytes 6148
  165.0 50.0 %all-to-all-start.3 = ((bf16[32,24,2048]{2,1,0:T(8,128)(2,1)}), bf16[32,24,2048]{2,1,0:T(8,128)(2,1)S(1)}, u32[]{:S(2)}, u32[]{:S(2)}) async-start(bf16[32,24,2048]{2,1,0:T(8,128)(2,1)} %bitcast.122), calls=%async_computation.3 | async-start | bytes 6291456 | tf_op jit(solution)/shard_map/all_to_all | solution.py:190
  215.1 15.7 %copy-start.1 = (f32[16]{0:T(128)S(1)}, f32[16]{0:T(128)}, u32[]{:S(2)}) copy-start(f32[16]{0:T(128)} %param.15) | copy-start | bytes 196
Sparse Core Ops, SparseCore 0:
  12.3 130.4 all-gather.1
where the time goes:
time: 238 us
  waiting for transfers between devices  92.8 us (39%)
  matrix products  37.2 us (16%)
  local copies, waits for them, and re-layouts  34.6 us (15%)
  other arithmetic  25.3 us (11%)
  starting transfers between devices  24.2 us (10%)
  between operations  14.4 us (6%)
  blocking collectives  6.26 us (3%)
  loops' own time  2.87 us (1%)
    all_gather x1, waiting for transfers between devices, rows_first(): filled, at, done = (lax.all_gather(both, axis, axis=0, tiled=True), 0, [])  46.6 us
    all_to_all x1, waiting for transfers between devices, body(): lax.all_to_all(expert_rows.reshape(ep_count, capacity, model_width), EP,...  35 us
    reduce_sum x1, other arithmetic, body(): expert_out = jnp.sum(weighted, 1).astype(jnp.bfloat16)  9.22 us
    all_to_all x1, starting transfers between devices, exchange_in_order(): filled = lax.all_to_all(filled, axes[k], k, k, tiled=True)  8.38 us
    all_to_all x1, starting transfers between devices, body(): lax.all_to_all(expert_rows.reshape(ep_count, capacity, model_width), EP,...  8.24 us
    all_to_all x1, waiting for transfers between devices, exchange_in_order(): filled = lax.all_to_all(filled, axes[k], k, k, tiled=True)  7.85 us
    dot_general x4, matrix products, one_block(): jnp.einsum('hgqk,khd->qhgd', attn_weights, pair_block[:, :, 1], preferred...  7.75 us
    gather x2, local copies, waits for them, and re-layouts, body(): jnp.take(returned.reshape(ep_count * capacity, model_width), slot_index,...  6.5 us
  transfers between devices with their start and end apart: 6, of which 4 were waited for; matrix products, arithmetic and copies ran while one was open for 31% of the time, Pallas kernels for 0%

commit v1 on v0

v1 whole, which is shorter than its diff:
```python
import functools

import jax
import jax.numpy as jnp
from jax import lax
from jax.experimental import pallas as pl
from jax.experimental.pallas import tpu as pltpu
from jax.sharding import PartitionSpec as P

MESH = pl.DeviceIdType.MESH
HEAD_DIM = 64
WINDOW = 128
CAP = 24
F32 = jnp.float32
BF16 = jnp.bfloat16
NEG_FILL = -1e30

GU_CHUNKS = 4
DOWN_CHUNKS = 4


def kernel(
    n_ep,
    n_tp,
    q_hbm,
    kv_hbm,
    sink_ref,
    ow_hbm,
    tok_hbm,
    gain_ref,
    routes_ref,
    rw_ref,
    g_hbm,
    u_hbm,
    d_hbm,
    mix_hbm,
    exp_hbm,
    q_v,
    kv_v,
    ow_v,
    tok_v,
    normed_v,
    slots_v,
    comb_v,
    out_v,
    arr_v,
    gu_v,
    down_v,
    hid_v,
    back_v,
    ret_v,
    att_v,
    attin_v,
    mix_v,
    eout_v,
    loc_sem,
    halo_ssem,
    halo_rsem,
    gu_ssem,
    gu_rsem,
    gur_ssem,
    gur_rsem,
    dn_ssem,
    dn_rsem,
    dnr_ssem,
    dnr_rsem,
    disp_sem,
    ret_ssem,
    ret_rsem,
    att_sem,
    fin_sem,
):
    ep = lax.axis_index("ep")
    tp = lax.axis_index("tp")
    right = lax.rem(tp + 1, n_tp)
    left = lax.rem(tp + n_tp - 1, n_tp)
    next_ep = lax.rem(ep + 1, n_ep)
    prev_ep = lax.rem(ep + n_ep - 1, n_ep)
    rows = q_v.shape[0]
    width = tok_v.shape[1]
    half = width // 2
    hid = gu_v.shape[3]
    dcol = width // DOWN_CHUNKS
    slot_rows = n_ep * CAP

    def local(src, dst, k):
        return pltpu.make_async_copy(src, dst, loc_sem.at[k])

    loads = [
        local(tok_hbm, tok_v, 0),
        local(q_hbm, q_v, 1),
        local(kv_hbm, kv_v.at[pl.ds(WINDOW, rows)], 2),
        local(g_hbm.at[0], gu_v.at[0, 0], 3),
        local(u_hbm.at[0], gu_v.at[0, 1], 4),
        local(ow_hbm, ow_v, 5),
    ]
    for c in range(DOWN_CHUNKS):
        loads.append(local(d_hbm.at[0, :, pl.ds(c * dcol, dcol)], down_v.at[c, pl.ds(0, hid)], 6 + c))
    for copy in loads:
        copy.start()

    barrier = pltpu.get_barrier_semaphore()

    @pl.loop(1, n_ep)
    def _(d):
        pl.semaphore_signal(
            barrier, inc=1, device_id=(lax.rem(ep + d, n_ep), tp), device_id_type=MESH
        )

    for j in range(1, n_tp):
        pl.semaphore_signal(
            barrier, inc=1, device_id=(ep, lax.rem(tp + j, n_tp)), device_id_type=MESH
        )
    pl.semaphore_wait(barrier, n_ep - 1 + n_tp - 1)

    def remote(src, dst, ssem, rsem, device):
        return pltpu.make_async_remote_copy(
            src_ref=src,
            dst_ref=dst,
            send_sem=ssem,
            recv_sem=rsem,
            device_id=device,
            device_id_type=MESH,
        )

    halos = [
        remote(
            kv_hbm.at[pl.ds(rows - WINDOW, WINDOW)],
            kv_v.at[pl.ds(0, WINDOW)],
            halo_ssem.at[0],
            halo_rsem.at[0],
            (next_ep, tp),
        ),
        remote(
            kv_hbm.at[pl.ds(0, WINDOW)],
            kv_v.at[pl.ds(WINDOW + rows, WINDOW)],
            halo_ssem.at[1],
            halo_rsem.at[1],
            (prev_ep, tp),
        ),
    ]
    for copy in halos:
        copy.start()

    def gu_own(side, k):
        which = k % 2
        part = (k // 2 + side) % 2
        src = (g_hbm, u_hbm)[which].at[0, pl.ds(part * half, half)]
        dst = gu_v.at[1 + side, which, pl.ds(part * half, half)]
        return remote(
            src, dst, gu_ssem.at[side, k], gu_rsem.at[side, k], (ep, (right, left)[side])
        )

    def gu_relay(side, k):
        src = gu_v.at[1 + side, k, pl.ds(side * half, half)]
        dst = gu_v.at[3, k, pl.ds(side * half, half)]
        return remote(
            src, dst, gur_ssem.at[side, k], gur_rsem.at[side, k], (ep, (right, left)[side])
        )

    def dn_own(side, c):
        src = d_hbm.at[0, :, pl.ds(c * dcol, dcol)]
        dst = down_v.at[c, pl.ds((1 + side) * hid, hid)]
        return remote(
            src, dst, dn_ssem.at[side, c], dn_rsem.at[side, c], (ep, (right, left)[side])
        )

    def dn_relay(side, c):
        at = side * (hid // 2)
        src = down_v.at[c, pl.ds((1 + side) * hid + at, hid // 2)]
        dst = down_v.at[c, pl.ds(3 * hid + at, hid // 2)]
        return remote(
            src, dst, dnr_ssem.at[side, c], dnr_rsem.at[side, c], (ep, (right, left)[side])
        )

    for k in range(GU_CHUNKS):
        for side in range(2):
            gu_own(side, k).start()

    loads[0].wait()

    @pl.loop(0, 8)
    def _(i):
        at = pl.ds(pl.multiple_of(i * 32, 32), 32)
        x = tok_v[at, :].astype(F32)
        x = x - jnp.mean(x, -1, keepdims=True)
        var = jnp.mean(x * x, -1, keepdims=True)
        normed_v[at, :] = (x * lax.rsqrt(var + 1e-06) * gain_ref[...]).astype(BF16)

    tokens = tok_v.shape[0]
    first = routes_ref[0:1, :]
    second = routes_ref[1:2, :]
    expert_ids = lax.broadcasted_iota(jnp.int32, (n_ep, tokens), 0)
    is_first = expert_ids == first
    is_second = expert_ids == second
    named = is_first | is_second
    before = (
        lax.broadcasted_iota(jnp.int32, (tokens, tokens), 0)
        < lax.broadcasted_iota(jnp.int32, (tokens, tokens), 1)
    ).astype(F32)
    named_f = named.astype(F32)
    rank = jnp.dot(named_f.astype(BF16), before.astype(BF16), preferred_element_type=F32)
    rank = jnp.where(named, rank, -1.0).astype(BF16)
    weight = jnp.where(is_first, rw_ref[0:1, :], 0.0) + jnp.where(is_second, rw_ref[1:2, :], 0.0)
    weight_hi = weight.astype(BF16)
    weight_lo = (weight - weight_hi.astype(F32)).astype(BF16)

    def slot_expert(shape, axis):
        slot = lax.broadcasted_iota(jnp.int32, shape, axis).astype(F32)
        expert = jnp.floor((slot + 0.5) * (1.0 / CAP))
        return expert, slot - expert * CAP

    expert, place = slot_expert((slot_rows, n_ep), 0)
    spread = (expert == lax.broadcasted_iota(jnp.int32, (slot_rows, n_ep), 1).astype(F32)).astype(
        F32
    )
    _, place_t = slot_expert((slot_rows, tokens), 0)
    ranks = jnp.dot(spread.astype(BF16), rank, preferred_element_type=F32)
    slots_v[...] = jnp.where(ranks == place_t, 1.0, 0.0).astype(BF16)

    per_block = 8 * CAP

    @pl.loop(0, slot_rows // per_block)
    def _(i):
        at = pl.ds(pl.multiple_of(i * per_block, per_block), per_block)
        picked = jnp.dot(slots_v[at, :], normed_v[...], preferred_element_type=F32)
        out_v[pl.ds(i * 8, 8)] = picked.astype(BF16).reshape(8, CAP, width)

    @pl.loop(1, n_ep)
    def _(d):
        to = lax.rem(ep + d, n_ep)
        remote(out_v.at[to], arr_v.at[ep], disp_sem.at[0], disp_sem.at[1], (to, tp)).start()

    arr_v[ep] = out_v[ep]

    expert_c = jnp.floor((lax.broadcasted_iota(jnp.int32, (n_ep, slot_rows), 1).astype(F32) + 0.5) * (1.0 / CAP))
    spread_t = (
        expert_c == lax.broadcasted_iota(jnp.int32, (n_ep, slot_rows), 0).astype(F32)
    ).astype(F32).astype(BF16)

    def over_slots(table):
        return lax.dot_general(
            table.astype(F32).T.astype(BF16),
            spread_t,
            (((1,), (0,)), ((), ())),
            preferred_element_type=F32,
        )

    _, place_c = slot_expert((tokens, slot_rows), 1)
    chosen = over_slots(rank) == place_c
    comb_v[0] = jnp.where(chosen, over_slots(weight_hi), 0.0).astype(BF16)
    comb_v[1] = jnp.where(chosen, over_slots(weight_lo), 0.0).astype(BF16)

    loads[1].wait()
    loads[2].wait()
    for copy in halos:
        copy.wait_recv()
    block = 128
    span = block + 2 * WINDOW
    heads = q_v.shape[1] // HEAD_DIM
    blocks_per_dest = rows // block // n_tp
    rel = lax.broadcasted_iota(jnp.int32, (block, span), 1) - lax.broadcasted_iota(
        jnp.int32, (block, span), 0
    )
    key_at = lax.broadcasted_iota(jnp.int32, (block, span), 1)
    seq_total = rows * n_ep

    @pl.loop(0, rows // block)
    def _(b):
        row = pl.multiple_of(b * block, block)
        q = q_v[pl.ds(row, block), :] * jnp.asarray(HEAD_DIM**-0.5, BF16)
        kv = kv_v[pl.ds(row, span), :]
        keys = kv[:, 0:HEAD_DIM]
        values = kv[:, HEAD_DIM : 2 * HEAD_DIM]
        key_pos = key_at + (ep * rows + row - WINDOW)
        allowed = (rel >= 0) & (rel <= 2 * WINDOW) & (key_pos >= 0) & (key_pos < seq_total)
        outs = []
        for h in range(heads):
            sink = sink_ref[tp * heads + h]
            scores = lax.dot_general(
                q[:, h * HEAD_DIM : (h + 1) * HEAD_DIM],
                keys,
                (((1,), (1,)), ((), ())),
                preferred_element_type=F32,
            )
            scores = jnp.where(allowed, scores, NEG_FILL)
            top = jnp.maximum(jnp.max(scores, -1, keepdims=True), sink)
            expo = jnp.exp(scores - top)
            denom = jnp.sum(expo, -1, keepdims=True) + jnp.exp(sink - top)
            mixed = jnp.dot(expo.astype(BF16), values, preferred_element_type=F32)
            outs.append((mixed / denom).astype(BF16))
        att_v[b // blocks_per_dest, pl.ds(pl.multiple_of(lax.rem(b, blocks_per_dest) * block, block), block), :] = (
            jnp.concatenate(outs, axis=1)
        )

    attin_v[tp] = att_v[tp]

    for k in range(2):
        for side in range(2):
            gu_own(side, k).wait_recv()
            gu_relay(side, k).start()
    for c in range(2):
        for side in range(2):
            dn_own(side, c).start()

    arrived = arr_v.at[pl.ds(0, n_ep - 1)]
    pltpu.make_async_copy(arrived, arrived, disp_sem.at[1]).wait()

    def widen(s):
        @pl.loop(0, slot_rows // per_block)
        def _(i):
            x = arr_v[pl.ds(i * 8, 8)].reshape(per_block, width)
            g = jnp.dot(x, gu_v[s, 0], preferred_element_type=F32)
            u = jnp.dot(x, gu_v[s, 1], preferred_element_type=F32)
            at = pl.ds(pl.multiple_of(i * per_block, per_block), per_block)
            hid_v[s, at, :] = (g / (1.0 + jnp.exp(-g)) * u).astype(BF16)

    loads[3].wait()
    loads[4].wait()
    widen(0)
    for k in range(2, GU_CHUNKS):
        for side in range(2):
            gu_own(side, k).wait_recv()

    @pl.loop(1, 3)
    def _(s):
        widen(s)

    for k in range(2):
        for side in range(2):
            gu_relay(side, k).wait_recv()
    widen(3)

    for c in range(DOWN_CHUNKS):
        for side in range(2):
            dn_own(side, c).wait_recv()
            dn_relay(side, c).start()
        if c + 2 < DOWN_CHUNKS:
            for side in range(2):
                dn_own(side, c + 2).start()
        if c == DOWN_CHUNKS - 1:
            for j in range(1, n_tp):
                to = lax.rem(tp + j, n_tp)
                remote(
                    att_v.at[to], attin_v.at[tp], att_sem.at[0], att_sem.at[1], (ep, to)
                ).start()
        loads[6 + c].wait()
        for side in range(2):
            dn_relay(side, c).wait_recv()

        @pl.loop(0, slot_rows // per_block)
        def _(i):
            at = pl.ds(pl.multiple_of(i * per_block, per_block), per_block)
            total = jnp.zeros((per_block, dcol), F32)
            for s in range(4):
                total = total + jnp.dot(
                    hid_v[s, at, :],
                    down_v[c, s * hid : (s + 1) * hid, :],
                    preferred_element_type=F32,
                )
            back_v[c, pl.ds(i * 8, 8)] = total.astype(BF16).reshape(8, CAP, dcol)

        @pl.loop(1, n_ep)
        def _(d):
            to = lax.rem(ep + d, n_ep)
            remote(
                back_v.at[c, to], ret_v.at[c, ep], ret_ssem.at[c], ret_rsem.at[c], (to, tp)
            ).start()

        ret_v[c, ep] = back_v[c, ep]

    def combine(c):
        got = ret_v.at[c, pl.ds(0, n_ep - 1)]
        pltpu.make_async_copy(got, got, ret_rsem.at[c]).wait()
        results = ret_v[c].reshape(slot_rows, dcol)
        total = jnp.dot(comb_v[0], results, preferred_element_type=F32) + jnp.dot(
            comb_v[1], results, preferred_element_type=F32
        )
        eout_v[c] = total.astype(BF16)
        pltpu.make_async_copy(
            eout_v.at[c], exp_hbm.at[:, pl.ds(c * dcol, dcol)], fin_sem.at[c]
        ).start()

    combine(0)
    combine(1)

    loads[5].wait()
    got = attin_v.at[pl.ds(0, n_tp - 1)]
    pltpu.make_async_copy(got, got, att_sem.at[1]).wait()
    mcol = mix_v.shape[2]
    head_cols = heads * HEAD_DIM

    def mix_out(c):
        return pltpu.make_async_copy(
            mix_v.at[c], mix_hbm.at[:, pl.ds(c * mcol, mcol)], fin_sem.at[DOWN_CHUNKS + c]
        )

    for c in range(mix_v.shape[0]):
        total = jnp.zeros((mix_v.shape[1], mcol), F32)
        for s in range(n_tp):
            total = total + jnp.dot(
                attin_v[s],
                ow_v[s * head_cols : (s + 1) * head_cols, c * mcol : (c + 1) * mcol],
                preferred_element_type=F32,
            )
        mix_v[c] = total.astype(BF16)
        mix_out(c).start()

    combine(2)
    combine(3)

    for c in range(DOWN_CHUNKS):
        pltpu.make_async_copy(
            eout_v.at[c], exp_hbm.at[:, pl.ds(c * dcol, dcol)], fin_sem.at[c]
        ).wait()
    for c in range(mix_v.shape[0]):
        mix_out(c).wait()
    for copy in halos:
        copy.wait_send()
    for side in range(2):
        for k in range(GU_CHUNKS):
            gu_own(side, k).wait_send()
        for k in range(2):
            gu_relay(side, k).wait_send()
        for c in range(DOWN_CHUNKS):
            dn_own(side, c).wait_send()
            dn_relay(side, c).wait_send()
    sent = out_v.at[pl.ds(0, n_ep - 1)]
    pltpu.make_async_copy(sent, sent, disp_sem.at[0]).wait()
    for c in range(DOWN_CHUNKS):
        sent = back_v.at[c, pl.ds(0, n_ep - 1)]
        pltpu.make_async_copy(sent, sent, ret_ssem.at[c]).wait()
    sent = att_v.at[pl.ds(0, n_tp - 1)]
    pltpu.make_async_copy(sent, sent, att_sem.at[0]).wait()


def body(
    queries,
    keys_values,
    sink_logits,
    out_weight,
    expert_tokens,
    norm_gain,
    routes,
    route_weights,
    gate_weight,
    up_weight,
    down_weight,
):
    n_ep = lax.axis_size("ep")
    n_tp = lax.axis_size("tp")
    rows, q_cols = queries.shape
    tokens, width = expert_tokens.shape
    hid = gate_weight.shape[2]
    out_rows = rows // n_tp
    dcol = width // DOWN_CHUNKS
    mcol = width // 4
    slot_rows = n_ep * CAP
    any_space = pl.BlockSpec(memory_space=pl.ANY)
    vmem = pl.BlockSpec(memory_space=pltpu.VMEM)
    smem = pl.BlockSpec(memory_space=pltpu.SMEM)
    dma = pltpu.SemaphoreType.DMA
    return pl.pallas_call(
        functools.partial(kernel, n_ep, n_tp),
        out_shape=(
            jax.ShapeDtypeStruct((out_rows, width), BF16),
            jax.ShapeDtypeStruct((tokens, width), BF16),
        ),
        in_specs=[
            any_space,
            any_space,
            smem,
            any_space,
            any_space,
            vmem,
            vmem,
            vmem,
            any_space,
            any_space,
            any_space,
        ],
        out_specs=(any_space, any_space),
        scratch_shapes=[
            pltpu.VMEM((rows, q_cols), BF16),
            pltpu.VMEM((rows + 2 * WINDOW, 2 * HEAD_DIM), BF16),
            pltpu.VMEM(out_weight.shape, BF16),
            pltpu.VMEM((tokens, width), BF16),
            pltpu.VMEM((tokens, width), BF16),
            pltpu.VMEM((slot_rows, tokens), BF16),
            pltpu.VMEM((2, tokens, slot_rows), BF16),
            pltpu.VMEM((n_ep, CAP, width), BF16),
            pltpu.VMEM((n_ep, CAP, width), BF16),
            pltpu.VMEM((4, 2, width, hid), BF16),
            pltpu.VMEM((DOWN_CHUNKS, 4 * hid, dcol), BF16),
            pltpu.VMEM((4, slot_rows, hid), BF16),
            pltpu.VMEM((DOWN_CHUNKS, n_ep, CAP, dcol), BF16),
            pltpu.VMEM((DOWN_CHUNKS, n_ep, CAP, dcol), BF16),
            pltpu.VMEM((n_tp, out_rows, q_cols), BF16),
            pltpu.VMEM((n_tp, out_rows, q_cols), BF16),
            pltpu.VMEM((4, out_rows, mcol), BF16),
            pltpu.VMEM((DOWN_CHUNKS, tokens, dcol), BF16),
            dma((6 + DOWN_CHUNKS,)),
            dma((2,)),
            dma((2,)),
            dma((2, GU_CHUNKS)),
            dma((2, GU_CHUNKS)),
            dma((2, 2)),
            dma((2, 2)),
            dma((2, DOWN_CHUNKS)),
            dma((2, DOWN_CHUNKS)),
            dma((2, DOWN_CHUNKS)),
            dma((2, DOWN_CHUNKS)),
            dma((2,)),
            dma((DOWN_CHUNKS,)),
            dma((DOWN_CHUNKS,)),
            dma((2,)),
            dma((DOWN_CHUNKS + 4,)),
        ],
        compiler_params=pltpu.CompilerParams(
            collective_id=0, has_side_effects=True, vmem_limit_bytes=60 * 1024 * 1024
        ),
    )(
        queries,
        keys_values,
        sink_logits,
        out_weight,
        expert_tokens,
        norm_gain.reshape(1, width),
        routes.T,
        route_weights.T,
        gate_weight,
        up_weight,
        down_weight,
    )


def solution(mesh):
    in_specs = (
        P("ep", "tp"),
        P("ep", "tp"),
        P(),
        P(),
        P(("ep", "tp"), None),
        P(),
        P(("ep", "tp"), None),
        P(("ep", "tp"), None),
        P("ep", None, "tp"),
        P("ep", None, "tp"),
        P("ep", "tp", None),
    )
    out_specs = (P(("ep", "tp"), None), P(("ep", "tp"), None))
    return jax.shard_map(body, mesh=mesh, in_specs=in_specs, out_specs=out_specs, check_vma=False)
```

time: 238 us -> 139 us (0.58)
  Pallas kernels: 0 us -> 133 us
  waiting for transfers between devices: 92.8 us -> 0 us
  matrix products: 37.2 us -> 0 us
  local copies, waits for them, and re-layouts: 34.6 us -> 4.22 us
  other arithmetic: 25.3 us -> 0 us
  starting transfers between devices: 24.2 us -> 0 us
  between operations: 14.4 us -> 0.65 us
  blocking collectives: 6.26 us -> 0 us
  loops' own time: 2.87 us -> 0 us
    pallas_call x0 -> x1, Pallas kernels: none -> 133 us  [body(): pl.pallas_call(functools.partial(kernel, n_ep, n_tp), out_shape=(jax.Shap...]
    all_gather x1 -> x0, waiting for transfers between devices: 46.6 us -> none  [rows_first(): filled, at, done = (lax.all_gather(both, axis, axis=0, tiled=True), 0, [])]
    all_to_all x3 -> x0, waiting for transfers between devices: 42.8 us -> none  [the longest x1 35 us: body(): lax.all_to_all(expert_rows.reshape(ep_count, capacity, model_width), EP,...]
    dot_general x12 -> x0, matrix products: 37.2 us -> none  [the longest x4 7.75 us: one_block(): jnp.einsum('hgqk,khd->qhgd', attn_weights, pair_block[:, :, 1], preferred...]
    all_to_all x3 -> x0, starting transfers between devices: 21.1 us -> none  [the longest x1 8.38 us: exchange_in_order(): filled = lax.all_to_all(filled, axes[k], k, k, tiled=True)]
    reduce_sum x8 -> x0, other arithmetic: 15.4 us -> none  [the longest x1 9.22 us: body(): expert_out = jnp.sum(weighted, 1).astype(jnp.bfloat16)]
    gather x3 -> x0, local copies, waits for them, and re-layouts: 10.8 us -> none  [the longest x2 6.5 us: body(): jnp.take(returned.reshape(ep_count * capacity, model_width), slot_index,...]
    dynamic_slice x16 -> x0, local copies, waits for them, and re-layouts: 6.99 us -> none  [the longest x8 4.48 us: one_block(): lax.dynamic_slice_in_dim(queries, first_row, block_rows, 0)]
  transfers between devices with their start and end apart: 6 -> 0, of which waited for: 4 -> 0; matrix products, arithmetic and copies ran while one was open for 31% -> 0% of each run, Pallas kernels for 0% -> 0%
where the time goes in v1:
time: 139 us; the launch traced here: 138 us
  Pallas kernels  133 us (96%)
  local copies, waits for them, and re-layouts  4.22 us (3%)
    pallas_call x1, Pallas kernels, body(): pl.pallas_call(functools.partial(kernel, n_ep, n_tp), out_shape=(jax.Shap...  133 us
    unnamed x4, local copies, waits for them, and re-layouts  4.22 us

profile of v1, /device:TPU:0, one launch (start us, length us, event | category | flops | bytes accessed | tf_op | source)
XLA Modules:
  0.0 137.8 jit_solution(8008540858633663294)
XLA Ops:
  0.6 132.9 %shard_map.122 = (bf16[512,2048]{1,0:T(8,128)(2,1)}, bf16[256,2048]{1,0:T(8,128)(2,1)}) custom-call(bf16[2048,256]{1,0:T(8,128)(2,1)} %q_hbm.1, bf16[2048,128]{1,0:T(8,128)(2,1)} %kv_hbm.1, f32[16]{0:T(128)} %sink_ref.1, bf16[1024,2048]{1,0:T(8,128)(2,1)} %ow_hbm.1, bf16[256,2048]{1,0:T(8,128)(2,1)} %tok_hbm.1, f32[1,2048]{1,0:T(1,128)} %bitcast.3, ...), custom_call_target="tpu_custom_call" | custom-call | tf_op jit(solution)/shard_map/pallas_call | solution.py:463
  133.5 0.0 copy-start
  133.5 3.2 %copy.15 = bf16[512,2048]{1,0:T(8,128)(2,1)} copy(bf16[512,2048]{1,0:T(8,128)(2,1)} %get-tuple-element.4) | data formatting | bytes 4194304
  136.8 0.0 copy-done
  136.8 1.0 copy.16
Async XLA Ops:
  133.5 3.3 %copy-start = (bf16[256,2048]{1,0:T(8,128)(2,1)S(1)}, bf16[256,2048]{1,0:T(8,128)(2,1)}, u32[]{:S(2)}) copy-start(bf16[256,2048]{1,0:T(8,128)(2,1)} %get-tuple-element.5) | copy-start | bytes 3145732

commit v2 on v1

--- a/solution.py
+++ b/solution.py
@@ -16,7 +16,8 @@
 NEG_FILL = -1e30
 
 GU_CHUNKS = 4
-DOWN_CHUNKS = 4
+DOWN_CHUNKS = 8
+ATT_PARTS = 4
 
 
 def kernel(
@@ -24,17 +25,21 @@
     n_tp,
     q_hbm,
     kv_hbm,
-    sink_ref,
+    sink_hbm,
     ow_hbm,
     tok_hbm,
+    gain_hbm,
+    routes_hbm,
+    rw_hbm,
+    g_hbm,
+    u_hbm,
+    d_hbm,
+    mix_ref,
+    exp_ref,
+    sink_ref,
     gain_ref,
     routes_ref,
     rw_ref,
-    g_hbm,
-    u_hbm,
-    d_hbm,
-    mix_hbm,
-    exp_hbm,
     q_v,
     kv_v,
     ow_v,
@@ -51,8 +56,7 @@
     ret_v,
     att_v,
     attin_v,
-    mix_v,
-    eout_v,
+    pass_v,
     loc_sem,
     halo_ssem,
     halo_rsem,
@@ -67,8 +71,12 @@
     disp_sem,
     ret_ssem,
     ret_rsem,
-    att_sem,
-    fin_sem,
+    far_ssem,
+    far_rsem,
+    fwd_ssem,
+    fwd_rsem,
+    att_ssem,
+    att_rsem,
 ):
     ep = lax.axis_index("ep")
     tp = lax.axis_index("tp")
@@ -93,25 +101,26 @@
         local(g_hbm.at[0], gu_v.at[0, 0], 3),
         local(u_hbm.at[0], gu_v.at[0, 1], 4),
         local(ow_hbm, ow_v, 5),
+        local(gain_hbm, gain_ref, 6),
+        local(routes_hbm, routes_ref, 7),
+        local(rw_hbm, rw_ref, 8),
+        local(sink_hbm, sink_ref, 9),
     ]
     for c in range(DOWN_CHUNKS):
-        loads.append(local(d_hbm.at[0, :, pl.ds(c * dcol, dcol)], down_v.at[c, pl.ds(0, hid)], 6 + c))
-    for copy in loads:
-        copy.start()
-
+        loads.append(local(d_hbm.at[0, :, pl.ds(c * dcol, dcol)], down_v.at[c, pl.ds(0, hid)], 10 + c))
     barrier = pltpu.get_barrier_semaphore()
+
+    def greet(semaphore, device):
+        pl.semaphore_signal(semaphore, inc=1, device_id=device, device_id_type=MESH)
+
+    greet(barrier, (ep, right))
+    greet(barrier, (ep, left))
 
     @pl.loop(1, n_ep)
     def _(d):
-        pl.semaphore_signal(
-            barrier, inc=1, device_id=(lax.rem(ep + d, n_ep), tp), device_id_type=MESH
-        )
-
-    for j in range(1, n_tp):
-        pl.semaphore_signal(
-            barrier, inc=1, device_id=(ep, lax.rem(tp + j, n_tp)), device_id_type=MESH
-        )
-    pl.semaphore_wait(barrier, n_ep - 1 + n_tp - 1)
+        greet(barrier, (lax.rem(ep + d, n_ep), tp))
+
+    pl.semaphore_wait(barrier, 2 + n_ep - 1)
 
     def remote(src, dst, ssem, rsem, device):
         return pltpu.make_async_remote_copy(
@@ -139,9 +148,6 @@
             (prev_ep, tp),
         ),
     ]
-    for copy in halos:
-        copy.start()
-
     def gu_own(side, k):
         which = k % 2
         part = (k // 2 + side) % 2
@@ -173,11 +179,46 @@
             src, dst, dnr_ssem.at[side, c], dnr_rsem.at[side, c], (ep, (right, left)[side])
         )
 
+    opposite = lax.rem(tp + 2, n_tp)
+    part_rows = att_v.shape[1] // ATT_PARTS
+    part_cols = att_v.shape[2] // 2
+
+    def att_far(side, p):
+        at = pl.ds(p * part_rows, part_rows)
+        src = att_v.at[opposite, at, pl.ds(side * part_cols, part_cols)]
+        dst = pass_v.at[side, p]
+        return remote(
+            src, dst, far_ssem.at[side, p], far_rsem.at[side, p], (ep, (right, left)[side])
+        )
+
+    def att_fwd(side, p):
+        at = pl.ds(p * part_rows, part_rows)
+        dst = attin_v.at[(left, right)[side], at, pl.ds(side * part_cols, part_cols)]
+        return remote(
+            pass_v.at[side, p],
+            dst,
+            fwd_ssem.at[side, p],
+            fwd_rsem.at[side, p],
+            (ep, (right, left)[side]),
+        )
+
+    def att_near(side, p):
+        at = pl.ds(p * part_rows, part_rows)
+        to = (right, left)[side]
+        return remote(
+            att_v.at[to, at], attin_v.at[tp, at], att_ssem.at[side, p], att_rsem.at[side, p], (ep, to)
+        )
+
     for k in range(GU_CHUNKS):
         for side in range(2):
             gu_own(side, k).start()
 
+    for copy in loads:
+        copy.start()
+
     loads[0].wait()
+    for k in range(6, 10):
+        loads[k].wait()
 
     @pl.loop(0, 8)
     def _(i):
@@ -226,13 +267,6 @@
         picked = jnp.dot(slots_v[at, :], normed_v[...], preferred_element_type=F32)
         out_v[pl.ds(i * 8, 8)] = picked.astype(BF16).reshape(8, CAP, width)
 
-    @pl.loop(1, n_ep)
-    def _(d):
-        to = lax.rem(ep + d, n_ep)
-        remote(out_v.at[to], arr_v.at[ep], disp_sem.at[0], disp_sem.at[1], (to, tp)).start()
-
-    arr_v[ep] = out_v[ep]
-
     expert_c = jnp.floor((lax.broadcasted_iota(jnp.int32, (n_ep, slot_rows), 1).astype(F32) + 0.5) * (1.0 / CAP))
     spread_t = (
         expert_c == lax.broadcasted_iota(jnp.int32, (n_ep, slot_rows), 0).astype(F32)
@@ -250,6 +284,16 @@
     chosen = over_slots(rank) == place_c
     comb_v[0] = jnp.where(chosen, over_slots(weight_hi), 0.0).astype(BF16)
     comb_v[1] = jnp.where(chosen, over_slots(weight_lo), 0.0).astype(BF16)
+
+    for copy in halos:
+        copy.start()
+
+    @pl.loop(1, n_ep)
+    def _(d):
+        to = lax.rem(ep + d, n_ep)
+        remote(out_v.at[to], arr_v.at[ep], disp_sem.at[0], disp_sem.at[1], (to, tp)).start()
+
+    arr_v[ep] = out_v[ep]
 
     loads[1].wait()
     loads[2].wait()
@@ -331,22 +375,35 @@
             gu_relay(side, k).wait_recv()
     widen(3)
 
-    for c in range(DOWN_CHUNKS):
+    def combine(c):
+        got = ret_v.at[c, pl.ds(0, n_ep - 1)]
+        pltpu.make_async_copy(got, got, ret_rsem.at[c]).wait()
+        results = ret_v[c].reshape(slot_rows, dcol)
+        total = jnp.dot(comb_v[0], results, preferred_element_type=F32) + jnp.dot(
+            comb_v[1], results, preferred_element_type=F32
+        )
+        exp_ref[:, c * dcol : (c + 1) * dcol] = total.astype(BF16)
+
+    def pass_on(c):
         for side in range(2):
             dn_own(side, c).wait_recv()
             dn_relay(side, c).start()
         if c + 2 < DOWN_CHUNKS:
             for side in range(2):
                 dn_own(side, c + 2).start()
-        if c == DOWN_CHUNKS - 1:
-            for j in range(1, n_tp):
-                to = lax.rem(tp + j, n_tp)
-                remote(
-                    att_v.at[to], attin_v.at[tp], att_sem.at[0], att_sem.at[1], (ep, to)
-                ).start()
-        loads[6 + c].wait()
+        if c + 1 == DOWN_CHUNKS:
+            for send in (att_far, att_near):
+                for p in range(ATT_PARTS):
+                    for side in range(2):
+                        send(side, p).start()
+
+    pass_on(0)
+    for c in range(DOWN_CHUNKS):
+        loads[10 + c].wait()
         for side in range(2):
             dn_relay(side, c).wait_recv()
+        if c + 1 < DOWN_CHUNKS:
+            pass_on(c + 1)
 
         @pl.loop(0, slot_rows // per_block)
         def _(i):
@@ -368,53 +425,42 @@
             ).start()
 
         ret_v[c, ep] = back_v[c, ep]
-
-    def combine(c):
-        got = ret_v.at[c, pl.ds(0, n_ep - 1)]
-        pltpu.make_async_copy(got, got, ret_rsem.at[c]).wait()
-        results = ret_v[c].reshape(slot_rows, dcol)
-        total = jnp.dot(comb_v[0], results, preferred_element_type=F32) + jnp.dot(
-            comb_v[1], results, preferred_element_type=F32
-        )
-        eout_v[c] = total.astype(BF16)
-        pltpu.make_async_copy(
-            eout_v.at[c], exp_hbm.at[:, pl.ds(c * dcol, dcol)], fin_sem.at[c]
-        ).start()
-
-    combine(0)
-    combine(1)
+        if 4 <= c < DOWN_CHUNKS - 1:
+            combine(c - 4)
+
+    for p in range(ATT_PARTS):
+        for side in range(2):
+            att_far(side, p).wait_recv()
+            att_fwd(side, p).start()
+    combine(DOWN_CHUNKS - 5)
 
     loads[5].wait()
-    got = attin_v.at[pl.ds(0, n_tp - 1)]
-    pltpu.make_async_copy(got, got, att_sem.at[1]).wait()
-    mcol = mix_v.shape[2]
     head_cols = heads * HEAD_DIM
-
-    def mix_out(c):
-        return pltpu.make_async_copy(
-            mix_v.at[c], mix_hbm.at[:, pl.ds(c * mcol, mcol)], fin_sem.at[DOWN_CHUNKS + c]
-        )
-
-    for c in range(mix_v.shape[0]):
-        total = jnp.zeros((mix_v.shape[1], mcol), F32)
-        for s in range(n_tp):
-            total = total + jnp.dot(
-                attin_v[s],
-                ow_v[s * head_cols : (s + 1) * head_cols, c * mcol : (c + 1) * mcol],
-                preferred_element_type=F32,
-            )
-        mix_v[c] = total.astype(BF16)
-        mix_out(c).start()
-
-    combine(2)
-    combine(3)
-
-    for c in range(DOWN_CHUNKS):
-        pltpu.make_async_copy(
-            eout_v.at[c], exp_hbm.at[:, pl.ds(c * dcol, dcol)], fin_sem.at[c]
-        ).wait()
-    for c in range(mix_v.shape[0]):
-        mix_out(c).wait()
+    mcol = mix_ref.shape[1] // 4
+
+    def project(p):
+        for side in range(2):
+            att_near(side, p).wait_recv()
+            att_fwd(side, p).wait_recv()
+        at = pl.ds(p * part_rows, part_rows)
+        for n in range(4):
+            total = jnp.zeros((part_rows, mcol), F32)
+            for s in range(n_tp):
+                total = total + jnp.dot(
+                    attin_v[s, at, :],
+                    ow_v[s * head_cols : (s + 1) * head_cols, n * mcol : (n + 1) * mcol],
+                    preferred_element_type=F32,
+                )
+            mix_ref[at, n * mcol : (n + 1) * mcol] = total.astype(BF16)
+
+    combine(DOWN_CHUNKS - 4)
+    combine(DOWN_CHUNKS - 3)
+    for p in range(ATT_PARTS - 1):
+        project(p)
+    combine(DOWN_CHUNKS - 2)
+    project(ATT_PARTS - 1)
+    combine(DOWN_CHUNKS - 1)
+
     for copy in halos:
         copy.wait_send()
     for side in range(2):
@@ -425,13 +471,15 @@
         for c in range(DOWN_CHUNKS):
             dn_own(side, c).wait_send()
             dn_relay(side, c).wait_send()
+        for p in range(ATT_PARTS):
+            att_far(side, p).wait_send()
+            att_fwd(side, p).wait_send()
+            att_near(side, p).wait_send()
     sent = out_v.at[pl.ds(0, n_ep - 1)]
     pltpu.make_async_copy(sent, sent, disp_sem.at[0]).wait()
     for c in range(DOWN_CHUNKS):
         sent = back_v.at[c, pl.ds(0, n_ep - 1)]
         pltpu.make_async_copy(sent, sent, ret_ssem.at[c]).wait()
-    sent = att_v.at[pl.ds(0, n_tp - 1)]
-    pltpu.make_async_copy(sent, sent, att_sem.at[0]).wait()
 
 
 def body(
@@ -454,33 +502,23 @@
     hid = gate_weight.shape[2]
     out_rows = rows // n_tp
     dcol = width // DOWN_CHUNKS
-    mcol = width // 4
     slot_rows = n_ep * CAP
-    any_space = pl.BlockSpec(memory_space=pl.ANY)
+    hbm = pl.BlockSpec(memory_space=pltpu.HBM)
     vmem = pl.BlockSpec(memory_space=pltpu.VMEM)
-    smem = pl.BlockSpec(memory_space=pltpu.SMEM)
     dma = pltpu.SemaphoreType.DMA
     return pl.pallas_call(
         functools.partial(kernel, n_ep, n_tp),
         out_shape=(
-            jax.ShapeDtypeStruct((out_rows, width), BF16),
-            jax.ShapeDtypeStruct((tokens, width), BF16),
+            pltpu.VMEM((out_rows, width), BF16),
+            pltpu.VMEM((tokens, width), BF16),
         ),
-        in_specs=[
-            any_space,
-            any_space,
-            smem,
-            any_space,
-            any_space,
-            vmem,
-            vmem,
-            vmem,
-            any_space,
-            any_space,
-            any_space,
-        ],
-        out_specs=(any_space, any_space),
+        in_specs=[hbm] * 11,
+        out_specs=(vmem, vmem),
         scratch_shapes=[
+            pltpu.SMEM(sink_logits.shape, F32),
+            pltpu.VMEM((1, width), F32),
+            pltpu.VMEM((2, tokens), jnp.int32),
+            pltpu.VMEM((2, tokens), F32),
             pltpu.VMEM((rows, q_cols), BF16),
             pltpu.VMEM((rows + 2 * WINDOW, 2 * HEAD_DIM), BF16),
             pltpu.VMEM(out_weight.shape, BF16),
@@ -497,9 +535,8 @@
             pltpu.VMEM((DOWN_CHUNKS, n_ep, CAP, dcol), BF16),
             pltpu.VMEM((n_tp, out_rows, q_cols), BF16),
             pltpu.VMEM((n_tp, out_rows, q_cols), BF16),
-            pltpu.VMEM((4, out_rows, mcol), BF16),
-            pltpu.VMEM((DOWN_CHUNKS, tokens, dcol), BF16),
-            dma((6 + DOWN_CHUNKS,)),
+            pltpu.VMEM((2, ATT_PARTS, out_rows // ATT_PARTS, q_cols // 2), BF16),
+            dma((10 + DOWN_CHUNKS,)),
             dma((2,)),
             dma((2,)),
             dma((2, GU_CHUNKS)),
@@ -513,24 +550,33 @@
             dma((2,)),
             dma((DOWN_CHUNKS,)),
             dma((DOWN_CHUNKS,)),
-            dma((2,)),
-            dma((DOWN_CHUNKS + 4,)),
+            dma((2, ATT_PARTS)),
+            dma((2, ATT_PARTS)),
+            dma((2, ATT_PARTS)),
+            dma((2, ATT_PARTS)),
+            dma((2, ATT_PARTS)),
+            dma((2, ATT_PARTS)),
         ],
         compiler_params=pltpu.CompilerParams(
-            collective_id=0, has_side_effects=True, vmem_limit_bytes=60 * 1024 * 1024
+            collective_id=0, has_side_effects=True, vmem_limit_bytes=44 * 1024 * 1024
         ),
     )(
-        queries,
-        keys_values,
-        sink_logits,
-        out_weight,
-        expert_tokens,
-        norm_gain.reshape(1, width),
-        routes.T,
-        route_weights.T,
-        gate_weight,
-        up_weight,
-        down_weight,
+        *(
+            pltpu.with_memory_space_constraint(a, pltpu.HBM)
+            for a in (
+                queries,
+                keys_values,
+                sink_logits,
+                out_weight,
+                expert_tokens,
+                norm_gain.reshape(1, width),
+                routes.T,
+                route_weights.T,
+                gate_weight,
+                up_weight,
+                down_weight,
+            )
+        )
     )
 
 

time: 139 us -> 132 us (0.950); the launches traced: 138 us -> 132 us
  Pallas kernels: 133 us -> 129 us
  local copies, waits for them, and re-layouts: 4.22 us -> 2.29 us
    pallas_call x1, Pallas kernels: 133 us -> 129 us  [body(): pl.pallas_call(functools.partial(kernel, n_ep, n_tp), out_shape=(pltpu.VM...]
    unnamed x4 -> x2, local copies, waits for them, and re-layouts: 4.22 us -> 2.29 us
where the time goes in v2:
time: 132 us
  Pallas kernels  129 us (98%)
  local copies, waits for them, and re-layouts  2.29 us (2%)
    pallas_call x1, Pallas kernels, body(): pl.pallas_call(functools.partial(kernel, n_ep, n_tp), out_shape=(pltpu.VM...  129 us

profile of v2, /device:TPU:0, one launch (start us, length us, event | category | flops | bytes accessed | tf_op | source)
XLA Modules:
  0.0 132.3 jit_solution(6080405777463859613)
XLA Ops:
  0.6 129.4 %shard_map.122 = (bf16[512,2048]{1,0:T(8,128)(2,1)S(1)}, bf16[256,2048]{1,0:T(8,128)(2,1)S(1)}) custom-call(bf16[2048,256]{1,0:T(8,128)(2,1)} %q_hbm.1, bf16[2048,128]{1,0:T(8,128)(2,1)} %kv_hbm.1, f32[16]{0:T(128)} %sink_hbm.1, bf16[1024,2048]{1,0:T(8,128)(2,1)} %ow_hbm.1, bf16[256,2048]{1,0:T(8,128)(2,1)} %tok_hbm.1, f32[1,2048]{1,0:T(1,128)} %bitcast.3, ...), custom_call_target="tpu_custom_call" | custom-call | tf_op jit(solution)/shard_map/pallas_call | solution.py:509
  130.0 1.3 copy.15
  131.3 1.0 copy.16

commit v3 on v2

--- a/solution.py
+++ b/solution.py
@@ -11,13 +11,16 @@
 HEAD_DIM = 64
 WINDOW = 128
 CAP = 24
+SIDE = 4
+STEP = 13
 F32 = jnp.float32
 BF16 = jnp.bfloat16
 NEG_FILL = -1e30
 
 GU_CHUNKS = 4
-DOWN_CHUNKS = 8
-ATT_PARTS = 4
+COLUMNS = (128, 128, 256, 256, 256, 256, 256, 256, 128, 128)
+DOWN_CHUNKS = len(COLUMNS)
+ATT_PARTS = 2
 
 
 def kernel(
@@ -57,6 +60,8 @@
     att_v,
     attin_v,
     pass_v,
+    acc_v,
+    news_sem,
     loc_sem,
     halo_ssem,
     halo_rsem,
@@ -88,8 +93,11 @@
     width = tok_v.shape[1]
     half = width // 2
     hid = gu_v.shape[3]
-    dcol = width // DOWN_CHUNKS
+    starts = [sum(COLUMNS[:c]) for c in range(DOWN_CHUNKS)]
     slot_rows = n_ep * CAP
+
+    def of_width(c):
+        return pl.ds(starts[c], COLUMNS[c])
 
     def local(src, dst, k):
         return pltpu.make_async_copy(src, dst, loc_sem.at[k])
@@ -107,20 +115,34 @@
         local(sink_hbm, sink_ref, 9),
     ]
     for c in range(DOWN_CHUNKS):
-        loads.append(local(d_hbm.at[0, :, pl.ds(c * dcol, dcol)], down_v.at[c, pl.ds(0, hid)], 10 + c))
+        loads.append(local(d_hbm.at[0, :, of_width(c)], down_v.at[c, pl.ds(0, hid), pl.ds(0, COLUMNS[c])], 10 + c))
     barrier = pltpu.get_barrier_semaphore()
 
     def greet(semaphore, device):
         pl.semaphore_signal(semaphore, inc=1, device_id=device, device_id_type=MESH)
 
+    def turn(device):
+        y = lax.rem(device // 2, SIDE)
+        return (device // (2 * SIDE) + jnp.minimum(y, SIDE - 2)) * n_ep + device
+
+    mine = turn(ep)
     greet(barrier, (ep, right))
     greet(barrier, (ep, left))
 
-    @pl.loop(1, n_ep)
-    def _(d):
-        greet(barrier, (lax.rem(ep + d, n_ep), tp))
-
-    pl.semaphore_wait(barrier, 2 + n_ep - 1)
+    def greet_later(d, count):
+        to = lax.rem(ep + d, n_ep)
+        later = turn(to) > mine
+
+        @pl.when(later)
+        def _():
+            greet(barrier, (to, tp))
+
+        return count + jnp.where(later, 1, 0)
+
+    later_count = lax.fori_loop(1, n_ep, greet_later, 0)
+    for copy in loads:
+        copy.start()
+    pl.semaphore_wait(barrier, 2 + n_ep - 1 - later_count)
 
     def remote(src, dst, ssem, rsem, device):
         return pltpu.make_async_remote_copy(
@@ -165,16 +187,16 @@
         )
 
     def dn_own(side, c):
-        src = d_hbm.at[0, :, pl.ds(c * dcol, dcol)]
-        dst = down_v.at[c, pl.ds((1 + side) * hid, hid)]
+        src = d_hbm.at[0, :, of_width(c)]
+        dst = down_v.at[c, pl.ds((1 + side) * hid, hid), pl.ds(0, COLUMNS[c])]
         return remote(
             src, dst, dn_ssem.at[side, c], dn_rsem.at[side, c], (ep, (right, left)[side])
         )
 
     def dn_relay(side, c):
         at = side * (hid // 2)
-        src = down_v.at[c, pl.ds((1 + side) * hid + at, hid // 2)]
-        dst = down_v.at[c, pl.ds(3 * hid + at, hid // 2)]
+        src = down_v.at[c, pl.ds((1 + side) * hid + at, hid // 2), pl.ds(0, COLUMNS[c])]
+        dst = down_v.at[c, pl.ds(3 * hid + at, hid // 2), pl.ds(0, COLUMNS[c])]
         return remote(
             src, dst, dnr_ssem.at[side, c], dnr_rsem.at[side, c], (ep, (right, left)[side])
         )
@@ -213,8 +235,13 @@
         for side in range(2):
             gu_own(side, k).start()
 
-    for copy in loads:
-        copy.start()
+    @pl.loop(1, n_ep)
+    def _(d):
+        to = lax.rem(ep + d, n_ep)
+
+        @pl.when(turn(to) < mine)
+        def _():
+            greet(news_sem, (to, tp))
 
     loads[0].wait()
     for k in range(6, 10):
@@ -267,6 +294,20 @@
         picked = jnp.dot(slots_v[at, :], normed_v[...], preferred_element_type=F32)
         out_v[pl.ds(i * 8, 8)] = picked.astype(BF16).reshape(8, CAP, width)
 
+    @pl.when(later_count > 0)
+    def _():
+        pl.semaphore_wait(news_sem, later_count)
+
+    for copy in halos:
+        copy.start()
+
+    @pl.loop(1, n_ep)
+    def _(d):
+        to = lax.rem(ep + d * STEP, n_ep)
+        remote(out_v.at[to], arr_v.at[ep], disp_sem.at[0], disp_sem.at[1], (to, tp)).start()
+
+    arr_v[ep] = out_v[ep]
+
     expert_c = jnp.floor((lax.broadcasted_iota(jnp.int32, (n_ep, slot_rows), 1).astype(F32) + 0.5) * (1.0 / CAP))
     spread_t = (
         expert_c == lax.broadcasted_iota(jnp.int32, (n_ep, slot_rows), 0).astype(F32)
@@ -285,20 +326,8 @@
     comb_v[0] = jnp.where(chosen, over_slots(weight_hi), 0.0).astype(BF16)
     comb_v[1] = jnp.where(chosen, over_slots(weight_lo), 0.0).astype(BF16)
 
-    for copy in halos:
-        copy.start()
-
-    @pl.loop(1, n_ep)
-    def _(d):
-        to = lax.rem(ep + d, n_ep)
-        remote(out_v.at[to], arr_v.at[ep], disp_sem.at[0], disp_sem.at[1], (to, tp)).start()
-
-    arr_v[ep] = out_v[ep]
-
     loads[1].wait()
     loads[2].wait()
-    for copy in halos:
-        copy.wait_recv()
     block = 128
     span = block + 2 * WINDOW
     heads = q_v.shape[1] // HEAD_DIM
@@ -309,8 +338,7 @@
     key_at = lax.broadcasted_iota(jnp.int32, (block, span), 1)
     seq_total = rows * n_ep
 
-    @pl.loop(0, rows // block)
-    def _(b):
+    def attend(b):
         row = pl.multiple_of(b * block, block)
         q = q_v[pl.ds(row, block), :] * jnp.asarray(HEAD_DIM**-0.5, BF16)
         kv = kv_v[pl.ds(row, span), :]
@@ -337,7 +365,18 @@
             jnp.concatenate(outs, axis=1)
         )
 
-    attin_v[tp] = att_v[tp]
+    blocks = rows // block
+
+    @pl.loop(1, blocks - 1)
+    def _(b):
+        attend(b)
+
+    for copy in halos:
+        copy.wait_recv()
+
+    @pl.loop(0, 2)
+    def _(i):
+        attend(i * (blocks - 1))
 
     for k in range(2):
         for side in range(2):
@@ -376,13 +415,27 @@
     widen(3)
 
     def combine(c):
-        got = ret_v.at[c, pl.ds(0, n_ep - 1)]
+        cols = COLUMNS[c]
+        got = ret_v.at[c, pl.ds(0, n_ep - 1), :, pl.ds(0, cols)]
         pltpu.make_async_copy(got, got, ret_rsem.at[c]).wait()
-        results = ret_v[c].reshape(slot_rows, dcol)
+        results = ret_v[c, :, :, 0:cols].reshape(slot_rows, cols)
         total = jnp.dot(comb_v[0], results, preferred_element_type=F32) + jnp.dot(
             comb_v[1], results, preferred_element_type=F32
         )
-        exp_ref[:, c * dcol : (c + 1) * dcol] = total.astype(BF16)
+        exp_ref[:, of_width(c)] = total.astype(BF16)
+
+    def down_sent(c):
+        for side in range(2):
+            dn_own(side, c).wait_send()
+            dn_relay(side, c).wait_send()
+
+    def returned(c):
+        sent = back_v.at[c, pl.ds(0, n_ep - 1), :, pl.ds(0, COLUMNS[c])]
+        pltpu.make_async_copy(sent, sent, ret_ssem.at[c]).wait()
+
+    def both_ways(send, p):
+        for side in range(2):
+            send(side, p).start()
 
     def pass_on(c):
         for side in range(2):
@@ -391,11 +444,12 @@
         if c + 2 < DOWN_CHUNKS:
             for side in range(2):
                 dn_own(side, c + 2).start()
+        if c + 2 == DOWN_CHUNKS:
+            both_ways(att_far, 0)
         if c + 1 == DOWN_CHUNKS:
-            for send in (att_far, att_near):
-                for p in range(ATT_PARTS):
-                    for side in range(2):
-                        send(side, p).start()
+            both_ways(att_far, 1)
+            for p in range(ATT_PARTS):
+                both_ways(att_near, p)
 
     pass_on(0)
     for c in range(DOWN_CHUNKS):
@@ -405,81 +459,106 @@
         if c + 1 < DOWN_CHUNKS:
             pass_on(c + 1)
 
+        cols = COLUMNS[c]
+        span_cols = pl.ds(0, cols)
+
         @pl.loop(0, slot_rows // per_block)
         def _(i):
             at = pl.ds(pl.multiple_of(i * per_block, per_block), per_block)
-            total = jnp.zeros((per_block, dcol), F32)
+            total = jnp.zeros((per_block, cols), F32)
             for s in range(4):
                 total = total + jnp.dot(
                     hid_v[s, at, :],
-                    down_v[c, s * hid : (s + 1) * hid, :],
+                    down_v[c, s * hid : (s + 1) * hid, 0:cols],
                     preferred_element_type=F32,
                 )
-            back_v[c, pl.ds(i * 8, 8)] = total.astype(BF16).reshape(8, CAP, dcol)
+            back_v[c, pl.ds(i * 8, 8), :, 0:cols] = total.astype(BF16).reshape(8, CAP, cols)
 
         @pl.loop(1, n_ep)
         def _(d):
-            to = lax.rem(ep + d, n_ep)
+            to = lax.rem(ep + d * STEP, n_ep)
             remote(
-                back_v.at[c, to], ret_v.at[c, ep], ret_ssem.at[c], ret_rsem.at[c], (to, tp)
+                back_v.at[c, to, :, span_cols],
+                ret_v.at[c, ep, :, span_cols],
+                ret_ssem.at[c],
+                ret_rsem.at[c],
+                (to, tp),
             ).start()
 
-        ret_v[c, ep] = back_v[c, ep]
-        if 4 <= c < DOWN_CHUNKS - 1:
-            combine(c - 4)
+        ret_v[c, ep, :, 0:cols] = back_v[c, ep, :, 0:cols]
+        if 5 <= c < DOWN_CHUNKS - 1:
+            combine(c - 5)
+        if c == 1:
+            for copy in halos:
+                copy.wait_send()
+            for side in range(2):
+                for k in range(GU_CHUNKS):
+                    gu_own(side, k).wait_send()
+                for k in range(2):
+                    gu_relay(side, k).wait_send()
+        if c == 2:
+            sent = out_v.at[pl.ds(0, n_ep - 1)]
+            pltpu.make_async_copy(sent, sent, disp_sem.at[0]).wait()
+        if c >= 3:
+            down_sent(c - 3)
 
     for p in range(ATT_PARTS):
         for side in range(2):
             att_far(side, p).wait_recv()
             att_fwd(side, p).start()
-    combine(DOWN_CHUNKS - 5)
+    for c in range(DOWN_CHUNKS - 3, DOWN_CHUNKS):
+        down_sent(c)
+    combine(DOWN_CHUNKS - 6)
+    for c in range(DOWN_CHUNKS - 5):
+        returned(c)
 
     loads[5].wait()
     head_cols = heads * HEAD_DIM
     mcol = mix_ref.shape[1] // 4
 
-    def project(p):
-        for side in range(2):
-            att_near(side, p).wait_recv()
-            att_fwd(side, p).wait_recv()
+    def add_heads(p, sources, first):
         at = pl.ds(p * part_rows, part_rows)
         for n in range(4):
-            total = jnp.zeros((part_rows, mcol), F32)
-            for s in range(n_tp):
+            cols = pl.ds(n * mcol, mcol)
+            total = jnp.zeros((part_rows, mcol), F32) if first else acc_v[at, cols]
+            for heads_of, source in sources:
                 total = total + jnp.dot(
-                    attin_v[s, at, :],
-                    ow_v[s * head_cols : (s + 1) * head_cols, n * mcol : (n + 1) * mcol],
+                    source[at, :],
+                    ow_v[pl.ds(pl.multiple_of(heads_of * head_cols, head_cols), head_cols), cols],
                     preferred_element_type=F32,
                 )
-            mix_ref[at, n * mcol : (n + 1) * mcol] = total.astype(BF16)
-
+            if first:
+                acc_v[at, cols] = total
+            else:
+                mix_ref[at, cols] = total.astype(BF16)
+
+    def project_near(p):
+        for side in range(2):
+            att_near(side, p).wait_recv()
+        add_heads(p, ((left, attin_v.at[left]), (right, attin_v.at[right]), (tp, att_v.at[tp])), True)
+
+    def project_far(p):
+        for side in range(2):
+            att_fwd(side, p).wait_recv()
+        add_heads(p, ((opposite, attin_v.at[opposite]),), False)
+
+    combine(DOWN_CHUNKS - 5)
+    project_near(0)
     combine(DOWN_CHUNKS - 4)
+    project_near(1)
     combine(DOWN_CHUNKS - 3)
-    for p in range(ATT_PARTS - 1):
-        project(p)
+    for p in range(ATT_PARTS):
+        project_far(p)
     combine(DOWN_CHUNKS - 2)
-    project(ATT_PARTS - 1)
-    combine(DOWN_CHUNKS - 1)
-
-    for copy in halos:
-        copy.wait_send()
+
     for side in range(2):
-        for k in range(GU_CHUNKS):
-            gu_own(side, k).wait_send()
-        for k in range(2):
-            gu_relay(side, k).wait_send()
-        for c in range(DOWN_CHUNKS):
-            dn_own(side, c).wait_send()
-            dn_relay(side, c).wait_send()
         for p in range(ATT_PARTS):
             att_far(side, p).wait_send()
             att_fwd(side, p).wait_send()
             att_near(side, p).wait_send()
-    sent = out_v.at[pl.ds(0, n_ep - 1)]
-    pltpu.make_async_copy(sent, sent, disp_sem.at[0]).wait()
-    for c in range(DOWN_CHUNKS):
-        sent = back_v.at[c, pl.ds(0, n_ep - 1)]
-        pltpu.make_async_copy(sent, sent, ret_ssem.at[c]).wait()
+    for c in range(DOWN_CHUNKS - 5, DOWN_CHUNKS):
+        returned(c)
+    combine(DOWN_CHUNKS - 1)
 
 
 def body(
@@ -501,7 +580,7 @@
     tokens, width = expert_tokens.shape
     hid = gate_weight.shape[2]
     out_rows = rows // n_tp
-    dcol = width // DOWN_CHUNKS
+    dcol = max(COLUMNS)
     slot_rows = n_ep * CAP
     hbm = pl.BlockSpec(memory_space=pltpu.HBM)
     vmem = pl.BlockSpec(memory_space=pltpu.VMEM)
@@ -536,6 +615,8 @@
             pltpu.VMEM((n_tp, out_rows, q_cols), BF16),
             pltpu.VMEM((n_tp, out_rows, q_cols), BF16),
             pltpu.VMEM((2, ATT_PARTS, out_rows // ATT_PARTS, q_cols // 2), BF16),
+            pltpu.VMEM((out_rows, width), F32),
+            pltpu.SemaphoreType.REGULAR,
             dma((10 + DOWN_CHUNKS,)),
             dma((2,)),
             dma((2,)),
@@ -558,7 +639,7 @@
             dma((2, ATT_PARTS)),
         ],
         compiler_params=pltpu.CompilerParams(
-            collective_id=0, has_side_effects=True, vmem_limit_bytes=44 * 1024 * 1024
+            collective_id=0, has_side_effects=True, vmem_limit_bytes=52 * 1024 * 1024
         ),
     )(
         *(

time: 132 us -> 133 us (level)
  no operation moved by 1% of the time
where the time goes in v3:
time: 133 us; the launch traced here: 132 us
  Pallas kernels  129 us (97%)
  local copies, waits for them, and re-layouts  2.29 us (2%)
    pallas_call x1, Pallas kernels, body(): pl.pallas_call(functools.partial(kernel, n_ep, n_tp), out_shape=(pltpu.VM...  129 us

profile of v3, /device:TPU:0, one launch (start us, length us, event | category | flops | bytes accessed | tf_op | source)
XLA Modules:
  0.0 132.0 jit_solution(17376635692400376332)
XLA Ops:
  0.6 129.1 %shard_map.122 = (bf16[512,2048]{1,0:T(8,128)(2,1)S(1)}, bf16[256,2048]{1,0:T(8,128)(2,1)S(1)}) custom-call(bf16[2048,256]{1,0:T(8,128)(2,1)} %q_hbm.1, bf16[2048,128]{1,0:T(8,128)(2,1)} %kv_hbm.1, f32[16]{0:T(128)} %sink_hbm.1, bf16[1024,2048]{1,0:T(8,128)(2,1)} %ow_hbm.1, bf16[256,2048]{1,0:T(8,128)(2,1)} %tok_hbm.1, f32[1,2048]{1,0:T(1,128)} %bitcast.3, ...), custom_call_target="tpu_custom_call" | custom-call | tf_op jit(solution)/shard_map/pallas_call | solution.py:588
  129.7 1.3 %copy.15 = bf16[512,2048]{1,0:T(8,128)(2,1)} copy(bf16[512,2048]{1,0:T(8,128)(2,1)S(1)} %get-tuple-element.2) | data formatting | bytes 4194304
  131.0 1.0 copy.16

commit v4 on v3

--- a/solution.py
+++ b/solution.py
@@ -18,7 +18,7 @@
 NEG_FILL = -1e30
 
 GU_CHUNKS = 4
-COLUMNS = (128, 128, 256, 256, 256, 256, 256, 256, 128, 128)
+COLUMNS = (256,) * 8
 DOWN_CHUNKS = len(COLUMNS)
 ATT_PARTS = 2
 
@@ -61,27 +61,20 @@
     attin_v,
     pass_v,
     acc_v,
+    silu_v,
     news_sem,
     loc_sem,
-    halo_ssem,
-    halo_rsem,
-    gu_ssem,
-    gu_rsem,
-    gur_ssem,
-    gur_rsem,
-    dn_ssem,
-    dn_rsem,
-    dnr_ssem,
-    dnr_rsem,
+    halo_sem,
+    sent_sem,
+    gu_sem,
+    gur_sem,
+    dn_sem,
+    dnr_sem,
     disp_sem,
-    ret_ssem,
-    ret_rsem,
-    far_ssem,
-    far_rsem,
-    fwd_ssem,
-    fwd_rsem,
-    att_ssem,
-    att_rsem,
+    ret_sem,
+    far_sem,
+    fwd_sem,
+    near_sem,
 ):
     ep = lax.axis_index("ep")
     tp = lax.axis_index("tp")
@@ -115,7 +108,7 @@
         local(sink_hbm, sink_ref, 9),
     ]
     for c in range(DOWN_CHUNKS):
-        loads.append(local(d_hbm.at[0, :, of_width(c)], down_v.at[c, pl.ds(0, hid), pl.ds(0, COLUMNS[c])], 10 + c))
+        loads.append(local(d_hbm.at[0, :, of_width(c)], down_v.at[c, pl.ds(0, hid), pl.ds(0, COLUMNS[c])], 10))
     barrier = pltpu.get_barrier_semaphore()
 
     def greet(semaphore, device):
@@ -154,19 +147,26 @@
             device_id_type=MESH,
         )
 
+    def take(like, semaphore):
+        pltpu.make_async_copy(like, like, semaphore).wait()
+
+    def both_ways(send, p):
+        for side in range(2):
+            send(side, p).start()
+
     halos = [
         remote(
             kv_hbm.at[pl.ds(rows - WINDOW, WINDOW)],
             kv_v.at[pl.ds(0, WINDOW)],
-            halo_ssem.at[0],
-            halo_rsem.at[0],
+            halo_sem.at[0],
+            halo_sem.at[1],
             (next_ep, tp),
         ),
         remote(
             kv_hbm.at[pl.ds(0, WINDOW)],
             kv_v.at[pl.ds(WINDOW + rows, WINDOW)],
-            halo_ssem.at[1],
-            halo_rsem.at[1],
+            halo_sem.at[0],
+            halo_sem.at[1],
             (prev_ep, tp),
         ),
     ]
@@ -176,21 +176,21 @@
         src = (g_hbm, u_hbm)[which].at[0, pl.ds(part * half, half)]
         dst = gu_v.at[1 + side, which, pl.ds(part * half, half)]
         return remote(
-            src, dst, gu_ssem.at[side, k], gu_rsem.at[side, k], (ep, (right, left)[side])
+            src, dst, sent_sem.at[0], gu_sem.at[k], (ep, (right, left)[side])
         )
 
     def gu_relay(side, k):
         src = gu_v.at[1 + side, k, pl.ds(side * half, half)]
         dst = gu_v.at[3, k, pl.ds(side * half, half)]
         return remote(
-            src, dst, gur_ssem.at[side, k], gur_rsem.at[side, k], (ep, (right, left)[side])
+            src, dst, sent_sem.at[1], gur_sem.at[k], (ep, (right, left)[side])
         )
 
     def dn_own(side, c):
         src = d_hbm.at[0, :, of_width(c)]
         dst = down_v.at[c, pl.ds((1 + side) * hid, hid), pl.ds(0, COLUMNS[c])]
         return remote(
-            src, dst, dn_ssem.at[side, c], dn_rsem.at[side, c], (ep, (right, left)[side])
+            src, dst, sent_sem.at[2], dn_sem.at[c], (ep, (right, left)[side])
         )
 
     def dn_relay(side, c):
@@ -198,7 +198,7 @@
         src = down_v.at[c, pl.ds((1 + side) * hid + at, hid // 2), pl.ds(0, COLUMNS[c])]
         dst = down_v.at[c, pl.ds(3 * hid + at, hid // 2), pl.ds(0, COLUMNS[c])]
         return remote(
-            src, dst, dnr_ssem.at[side, c], dnr_rsem.at[side, c], (ep, (right, left)[side])
+            src, dst, sent_sem.at[3], dnr_sem.at[c], (ep, (right, left)[side])
         )
 
     opposite = lax.rem(tp + 2, n_tp)
@@ -210,7 +210,7 @@
         src = att_v.at[opposite, at, pl.ds(side * part_cols, part_cols)]
         dst = pass_v.at[side, p]
         return remote(
-            src, dst, far_ssem.at[side, p], far_rsem.at[side, p], (ep, (right, left)[side])
+            src, dst, sent_sem.at[4], far_sem.at[p], (ep, (right, left)[side])
         )
 
     def att_fwd(side, p):
@@ -219,8 +219,8 @@
         return remote(
             pass_v.at[side, p],
             dst,
-            fwd_ssem.at[side, p],
-            fwd_rsem.at[side, p],
+            sent_sem.at[5],
+            fwd_sem.at[p],
             (ep, (right, left)[side]),
         )
 
@@ -228,12 +228,12 @@
         at = pl.ds(p * part_rows, part_rows)
         to = (right, left)[side]
         return remote(
-            att_v.at[to, at], attin_v.at[tp, at], att_ssem.at[side, p], att_rsem.at[side, p], (ep, to)
+            att_v.at[to, at], attin_v.at[tp, at], sent_sem.at[6], near_sem.at[p], (ep, to)
         )
 
     for k in range(GU_CHUNKS):
-        for side in range(2):
-            gu_own(side, k).start()
+        both_ways(gu_own, k)
+    both_ways(dn_own, 0)
 
     @pl.loop(1, n_ep)
     def _(d):
@@ -371,26 +371,32 @@
     def _(b):
         attend(b)
 
-    for copy in halos:
-        copy.wait_recv()
+    halo_like = kv_v.at[pl.ds(0, 2 * WINDOW)]
+    take(halo_like, halo_sem.at[1])
 
     @pl.loop(0, 2)
     def _(i):
         attend(i * (blocks - 1))
 
     for k in range(2):
-        for side in range(2):
-            gu_own(side, k).wait_recv()
-            gu_relay(side, k).start()
-    for c in range(2):
-        for side in range(2):
-            dn_own(side, c).start()
+        take(gu_v.at[1, 0], gu_sem.at[k])
+        both_ways(gu_relay, k)
 
     arrived = arr_v.at[pl.ds(0, n_ep - 1)]
     pltpu.make_async_copy(arrived, arrived, disp_sem.at[1]).wait()
 
+    slot_blocks = slot_rows // per_block
+
+    def pass_on(c):
+        take(down_v.at[c, pl.ds(hid, 2 * hid), pl.ds(0, COLUMNS[c])], dn_sem.at[c])
+        both_ways(dn_relay, c)
+        if c == 0:
+            both_ways(dn_own, 1)
+        if c + 2 < DOWN_CHUNKS:
+            both_ways(dn_own, c + 2)
+
     def widen(s):
-        @pl.loop(0, slot_rows // per_block)
+        @pl.loop(0, slot_blocks)
         def _(i):
             x = arr_v[pl.ds(i * 8, 8)].reshape(per_block, width)
             g = jnp.dot(x, gu_v[s, 0], preferred_element_type=F32)
@@ -402,62 +408,53 @@
     loads[4].wait()
     widen(0)
     for k in range(2, GU_CHUNKS):
-        for side in range(2):
-            gu_own(side, k).wait_recv()
+        take(gu_v.at[1, 0], gu_sem.at[k])
+
+    pass_on(0)
 
     @pl.loop(1, 3)
     def _(s):
         widen(s)
 
-    for k in range(2):
-        for side in range(2):
-            gu_relay(side, k).wait_recv()
-    widen(3)
+    take(gu_v.at[3, 0], gur_sem.at[0])
+
+    @pl.loop(0, slot_blocks)
+    def _(i):
+        x = arr_v[pl.ds(i * 8, 8)].reshape(per_block, width)
+        g = jnp.dot(x, gu_v[3, 0], preferred_element_type=F32)
+        at = pl.ds(pl.multiple_of(i * per_block, per_block), per_block)
+        silu_v[at, :] = g / (1.0 + jnp.exp(-g))
+
+    take(halo_like, halo_sem.at[0])
+    take(gu_v.at[pl.ds(0, 2)], sent_sem.at[0])
+    sent = out_v.at[pl.ds(0, n_ep - 1)]
+    take(sent, disp_sem.at[0])
+    take(gu_v.at[0, 0], loc_sem.at[10])
+    take(gu_v.at[3, 1], gur_sem.at[1])
+
+    @pl.loop(0, slot_blocks)
+    def _(i):
+        x = arr_v[pl.ds(i * 8, 8)].reshape(per_block, width)
+        u = jnp.dot(x, gu_v[3, 1], preferred_element_type=F32)
+        at = pl.ds(pl.multiple_of(i * per_block, per_block), per_block)
+        hid_v[3, at, :] = (silu_v[at, :] * u).astype(BF16)
+
+    take(gu_v.at[0], sent_sem.at[1])
 
     def combine(c):
         cols = COLUMNS[c]
         got = ret_v.at[c, pl.ds(0, n_ep - 1), :, pl.ds(0, cols)]
-        pltpu.make_async_copy(got, got, ret_rsem.at[c]).wait()
+        take(got, ret_sem.at[c])
         results = ret_v[c, :, :, 0:cols].reshape(slot_rows, cols)
         total = jnp.dot(comb_v[0], results, preferred_element_type=F32) + jnp.dot(
             comb_v[1], results, preferred_element_type=F32
         )
         exp_ref[:, of_width(c)] = total.astype(BF16)
 
-    def down_sent(c):
-        for side in range(2):
-            dn_own(side, c).wait_send()
-            dn_relay(side, c).wait_send()
-
-    def returned(c):
-        sent = back_v.at[c, pl.ds(0, n_ep - 1), :, pl.ds(0, COLUMNS[c])]
-        pltpu.make_async_copy(sent, sent, ret_ssem.at[c]).wait()
-
-    def both_ways(send, p):
-        for side in range(2):
-            send(side, p).start()
-
-    def pass_on(c):
-        for side in range(2):
-            dn_own(side, c).wait_recv()
-            dn_relay(side, c).start()
-        if c + 2 < DOWN_CHUNKS:
-            for side in range(2):
-                dn_own(side, c + 2).start()
-        if c + 2 == DOWN_CHUNKS:
-            both_ways(att_far, 0)
-        if c + 1 == DOWN_CHUNKS:
-            both_ways(att_far, 1)
-            for p in range(ATT_PARTS):
-                both_ways(att_near, p)
-
-    pass_on(0)
     for c in range(DOWN_CHUNKS):
-        loads[10 + c].wait()
-        for side in range(2):
-            dn_relay(side, c).wait_recv()
-        if c + 1 < DOWN_CHUNKS:
+        if 0 < c < DOWN_CHUNKS - 1:
             pass_on(c + 1)
+        take(down_v.at[c, pl.ds(3 * hid, hid), pl.ds(0, COLUMNS[c])], dnr_sem.at[c])
 
         cols = COLUMNS[c]
         span_cols = pl.ds(0, cols)
@@ -480,37 +477,26 @@
             remote(
                 back_v.at[c, to, :, span_cols],
                 ret_v.at[c, ep, :, span_cols],
-                ret_ssem.at[c],
-                ret_rsem.at[c],
+                sent_sem.at[7],
+                ret_sem.at[c],
                 (to, tp),
             ).start()
 
         ret_v[c, ep, :, 0:cols] = back_v[c, ep, :, 0:cols]
-        if 5 <= c < DOWN_CHUNKS - 1:
-            combine(c - 5)
-        if c == 1:
-            for copy in halos:
-                copy.wait_send()
-            for side in range(2):
-                for k in range(GU_CHUNKS):
-                    gu_own(side, k).wait_send()
-                for k in range(2):
-                    gu_relay(side, k).wait_send()
-        if c == 2:
-            sent = out_v.at[pl.ds(0, n_ep - 1)]
-            pltpu.make_async_copy(sent, sent, disp_sem.at[0]).wait()
-        if c >= 3:
-            down_sent(c - 3)
+        if c == 0:
+            pass_on(1)
+        if c == DOWN_CHUNKS - 2:
+            for send in (att_far, att_near):
+                for p in range(ATT_PARTS):
+                    both_ways(send, p)
+        if 4 <= c < DOWN_CHUNKS - 1:
+            combine(c - 4)
 
     for p in range(ATT_PARTS):
-        for side in range(2):
-            att_far(side, p).wait_recv()
-            att_fwd(side, p).start()
-    for c in range(DOWN_CHUNKS - 3, DOWN_CHUNKS):
-        down_sent(c)
-    combine(DOWN_CHUNKS - 6)
-    for c in range(DOWN_CHUNKS - 5):
-        returned(c)
+        take(pass_v.at[:, p], far_sem.at[p])
+        both_ways(att_fwd, p)
+    take(gu_v.at[0], sent_sem.at[2])
+    take(gu_v.at[0, 0], sent_sem.at[3])
 
     loads[5].wait()
     head_cols = heads * HEAD_DIM
@@ -533,13 +519,11 @@
                 mix_ref[at, cols] = total.astype(BF16)
 
     def project_near(p):
-        for side in range(2):
-            att_near(side, p).wait_recv()
+        take(attin_v.at[pl.ds(0, 2), pl.ds(p * part_rows, part_rows)], near_sem.at[p])
         add_heads(p, ((left, attin_v.at[left]), (right, attin_v.at[right]), (tp, att_v.at[tp])), True)
 
     def project_far(p):
-        for side in range(2):
-            att_fwd(side, p).wait_recv()
+        take(attin_v.at[opposite, pl.ds(p * part_rows, part_rows)], fwd_sem.at[p])
         add_heads(p, ((opposite, attin_v.at[opposite]),), False)
 
     combine(DOWN_CHUNKS - 5)
@@ -551,14 +535,22 @@
         project_far(p)
     combine(DOWN_CHUNKS - 2)
 
-    for side in range(2):
-        for p in range(ATT_PARTS):
-            att_far(side, p).wait_send()
-            att_fwd(side, p).wait_send()
-            att_near(side, p).wait_send()
-    for c in range(DOWN_CHUNKS - 5, DOWN_CHUNKS):
-        returned(c)
+    take(attin_v.at[0], sent_sem.at[4])
+    take(attin_v.at[0], sent_sem.at[5])
+    take(attin_v.at[pl.ds(0, 2)], sent_sem.at[6])
     combine(DOWN_CHUNKS - 1)
+    take(sent, sent_sem.at[7])
+
+
+def put_out(mix_ref, exp_ref, mix_hbm, exp_hbm, sem):
+    copies = [
+        pltpu.make_async_copy(mix_ref, mix_hbm, sem.at[0]),
+        pltpu.make_async_copy(exp_ref, exp_hbm, sem.at[1]),
+    ]
+    for copy in copies:
+        copy.start()
+    for copy in copies:
+        copy.wait()
 
 
 def body(
@@ -585,7 +577,7 @@
     hbm = pl.BlockSpec(memory_space=pltpu.HBM)
     vmem = pl.BlockSpec(memory_space=pltpu.VMEM)
     dma = pltpu.SemaphoreType.DMA
-    return pl.pallas_call(
+    held = pl.pallas_call(
         functools.partial(kernel, n_ep, n_tp),
         out_shape=(
             pltpu.VMEM((out_rows, width), BF16),
@@ -616,27 +608,20 @@
             pltpu.VMEM((n_tp, out_rows, q_cols), BF16),
             pltpu.VMEM((2, ATT_PARTS, out_rows // ATT_PARTS, q_cols // 2), BF16),
             pltpu.VMEM((out_rows, width), F32),
+            pltpu.VMEM((slot_rows, hid), F32),
             pltpu.SemaphoreType.REGULAR,
-            dma((10 + DOWN_CHUNKS,)),
+            dma((11,)),
             dma((2,)),
-            dma((2,)),
-            dma((2, GU_CHUNKS)),
-            dma((2, GU_CHUNKS)),
-            dma((2, 2)),
-            dma((2, 2)),
-            dma((2, DOWN_CHUNKS)),
-            dma((2, DOWN_CHUNKS)),
-            dma((2, DOWN_CHUNKS)),
-            dma((2, DOWN_CHUNKS)),
+            dma((8,)),
+            dma((GU_CHUNKS,)),
             dma((2,)),
             dma((DOWN_CHUNKS,)),
             dma((DOWN_CHUNKS,)),
-            dma((2, ATT_PARTS)),
-            dma((2, ATT_PARTS)),
-            dma((2, ATT_PARTS)),
-            dma((2, ATT_PARTS)),
-            dma((2, ATT_PARTS)),
-            dma((2, ATT_PARTS)),
+            dma((2,)),
+            dma((DOWN_CHUNKS,)),
+            dma((ATT_PARTS,)),
+            dma((ATT_PARTS,)),
+            dma((ATT_PARTS,)),
         ],
         compiler_params=pltpu.CompilerParams(
             collective_id=0, has_side_effects=True, vmem_limit_bytes=52 * 1024 * 1024
@@ -659,6 +644,17 @@
             )
         )
     )
+    return pl.pallas_call(
+        put_out,
+        out_shape=(
+            jax.ShapeDtypeStruct((out_rows, width), BF16),
+            jax.ShapeDtypeStruct((tokens, width), BF16),
+        ),
+        in_specs=[vmem, vmem],
+        out_specs=(pl.BlockSpec(memory_space=pl.ANY),) * 2,
+        scratch_shapes=[dma((2,))],
+        compiler_params=pltpu.CompilerParams(vmem_limit_bytes=1024 * 1024),
+    )(*held)
 
 
 def solution(mesh):

time: 133 us -> 126 us (0.947)
  Pallas kernels: 129 us -> 125 us
  local copies, waits for them, and re-layouts: 2.29 us -> 0 us
    pallas_call x1, Pallas kernels: 129 us -> 123 us  [body(): pl.pallas_call(functools.partial(kernel, n_ep, n_tp), out_shape=(pltpu.VM...]
    unnamed x2 -> x0, local copies, waits for them, and re-layouts: 2.29 us -> none
    pallas_call x0 -> x1, Pallas kernels: none -> 1.68 us  [body(): pl.pallas_call(put_out, out_shape=(jax.ShapeDtypeStruct((out_rows, width)...]
where the time goes in v4:
time: 126 us
  Pallas kernels  125 us (99%)
    pallas_call x1, Pallas kernels, body(): pl.pallas_call(functools.partial(kernel, n_ep, n_tp), out_shape=(pltpu.VM...  123 us

profile of v4, /device:TPU:0, one launch (start us, length us, event | category | flops | bytes accessed | tf_op | source)
XLA Modules:
  0.0 125.8 jit_solution(12135276821913613196)
XLA Ops:
  0.6 123.5 %shard_map.122 = (bf16[512,2048]{1,0:T(8,128)(2,1)S(1)}, bf16[256,2048]{1,0:T(8,128)(2,1)S(1)}) custom-call(bf16[2048,256]{1,0:T(8,128)(2,1)} %q_hbm.1, bf16[2048,128]{1,0:T(8,128)(2,1)} %kv_hbm.1, f32[16]{0:T(128)} %sink_hbm.1, bf16[1024,2048]{1,0:T(8,128)(2,1)} %ow_hbm.1, bf16[256,2048]{1,0:T(8,128)(2,1)} %tok_hbm.1, f32[1,2048]{1,0:T(1,128)} %bitcast.3, ...), custom_call_target="tpu_custom_call" | custom-call | tf_op jit(solution)/shard_map/pallas_call | solution.py:580
  124.1 1.7 %shard_map.123 = (bf16[512,2048]{1,0:T(8,128)(2,1)}, bf16[256,2048]{1,0:T(8,128)(2,1)}) custom-call(bf16[512,2048]{1,0:T(8,128)(2,1)S(1)} %get-tuple-element.4.mix_ref, bf16[256,2048]{1,0:T(8,128)(2,1)S(1)} %get-tuple-element.5.exp_ref), custom_call_target="tpu_custom_call" | custom-call | tf_op jit(solution)/shard_map/pallas_call | solution.py:647

commit v5 on v4

--- a/solution.py
+++ b/solution.py
@@ -62,6 +62,9 @@
     pass_v,
     acc_v,
     silu_v,
+    part_v,
+    sum_v,
+    got_v,
     news_sem,
     loc_sem,
     halo_sem,
@@ -75,6 +78,8 @@
     far_sem,
     fwd_sem,
     near_sem,
+    tok_sem,
+    part_sem,
 ):
     ep = lax.axis_index("ep")
     tp = lax.axis_index("tp")
@@ -83,11 +88,18 @@
     next_ep = lax.rem(ep + 1, n_ep)
     prev_ep = lax.rem(ep + n_ep - 1, n_ep)
     rows = q_v.shape[0]
-    width = tok_v.shape[1]
+    width = tok_v.shape[2]
+    parity = lax.rem(tp, 2)
+    at_site = lax.rem(ep, 2) == parity
+    off_site = lax.rem(ep, 2) != parity
+    partner = jnp.where(at_site, right, left)
+    served = n_ep // 2
+    place = ep // 2
     half = width // 2
     hid = gu_v.shape[3]
     starts = [sum(COLUMNS[:c]) for c in range(DOWN_CHUNKS)]
-    slot_rows = n_ep * CAP
+    slot_rows = 2 * n_ep * CAP
+    table_rows = served * CAP
 
     def of_width(c):
         return pl.ds(starts[c], COLUMNS[c])
@@ -96,15 +108,15 @@
         return pltpu.make_async_copy(src, dst, loc_sem.at[k])
 
     loads = [
-        local(tok_hbm, tok_v, 0),
+        local(tok_hbm, tok_v.at[0], 0),
         local(q_hbm, q_v, 1),
         local(kv_hbm, kv_v.at[pl.ds(WINDOW, rows)], 2),
         local(g_hbm.at[0], gu_v.at[0, 0], 3),
         local(u_hbm.at[0], gu_v.at[0, 1], 4),
         local(ow_hbm, ow_v, 5),
         local(gain_hbm, gain_ref, 6),
-        local(routes_hbm, routes_ref, 7),
-        local(rw_hbm, rw_ref, 8),
+        local(routes_hbm, routes_ref.at[0], 7),
+        local(rw_hbm, rw_ref.at[0], 8),
         local(sink_hbm, sink_ref, 9),
     ]
     for c in range(DOWN_CHUNKS):
@@ -193,6 +205,12 @@
             src, dst, sent_sem.at[2], dn_sem.at[c], (ep, (right, left)[side])
         )
 
+    def dn_half(side, c):
+        at = side * (hid // 2)
+        src = d_hbm.at[0, pl.ds(at, hid // 2), of_width(c)]
+        dst = down_v.at[c, pl.ds((1 + side) * hid + at, hid // 2), pl.ds(0, COLUMNS[c])]
+        return remote(src, dst, sent_sem.at[2], dn_sem.at[c], (ep, (right, left)[side]))
+
     def dn_relay(side, c):
         at = side * (hid // 2)
         src = down_v.at[c, pl.ds((1 + side) * hid + at, hid // 2), pl.ds(0, COLUMNS[c])]
@@ -231,10 +249,13 @@
             att_v.at[to, at], attin_v.at[tp, at], sent_sem.at[6], near_sem.at[p], (ep, to)
         )
 
-    for k in range(GU_CHUNKS):
-        both_ways(gu_own, k)
-    both_ways(dn_own, 0)
-
+    exchange = [
+        remote(routes_hbm, routes_ref.at[1], sent_sem.at[8], tok_sem.at[0], (ep, partner)),
+        remote(rw_hbm, rw_ref.at[1], sent_sem.at[9], tok_sem.at[1], (ep, partner)),
+        remote(tok_hbm, tok_v.at[1], sent_sem.at[10], tok_sem.at[2], (ep, partner)),
+    ]
+    for copy in exchange:
+        copy.start()
     @pl.loop(1, n_ep)
     def _(d):
         to = lax.rem(ep + d, n_ep)
@@ -243,56 +264,90 @@
         def _():
             greet(news_sem, (to, tp))
 
-    loads[0].wait()
-    for k in range(6, 10):
-        loads[k].wait()
-
-    @pl.loop(0, 8)
-    def _(i):
-        at = pl.ds(pl.multiple_of(i * 32, 32), 32)
-        x = tok_v[at, :].astype(F32)
-        x = x - jnp.mean(x, -1, keepdims=True)
-        var = jnp.mean(x * x, -1, keepdims=True)
-        normed_v[at, :] = (x * lax.rsqrt(var + 1e-06) * gain_ref[...]).astype(BF16)
-
-    tokens = tok_v.shape[0]
-    first = routes_ref[0:1, :]
-    second = routes_ref[1:2, :]
-    expert_ids = lax.broadcasted_iota(jnp.int32, (n_ep, tokens), 0)
-    is_first = expert_ids == first
-    is_second = expert_ids == second
-    named = is_first | is_second
-    before = (
-        lax.broadcasted_iota(jnp.int32, (tokens, tokens), 0)
-        < lax.broadcasted_iota(jnp.int32, (tokens, tokens), 1)
-    ).astype(F32)
-    named_f = named.astype(F32)
-    rank = jnp.dot(named_f.astype(BF16), before.astype(BF16), preferred_element_type=F32)
-    rank = jnp.where(named, rank, -1.0).astype(BF16)
-    weight = jnp.where(is_first, rw_ref[0:1, :], 0.0) + jnp.where(is_second, rw_ref[1:2, :], 0.0)
-    weight_hi = weight.astype(BF16)
-    weight_lo = (weight - weight_hi.astype(F32)).astype(BF16)
+    tokens = tok_v.shape[1]
+    per_block = 8 * CAP
 
     def slot_expert(shape, axis):
         slot = lax.broadcasted_iota(jnp.int32, shape, axis).astype(F32)
         expert = jnp.floor((slot + 0.5) * (1.0 / CAP))
         return expert, slot - expert * CAP
 
-    expert, place = slot_expert((slot_rows, n_ep), 0)
-    spread = (expert == lax.broadcasted_iota(jnp.int32, (slot_rows, n_ep), 1).astype(F32)).astype(
-        F32
-    )
-    _, place_t = slot_expert((slot_rows, tokens), 0)
-    ranks = jnp.dot(spread.astype(BF16), rank, preferred_element_type=F32)
-    slots_v[...] = jnp.where(ranks == place_t, 1.0, 0.0).astype(BF16)
-
-    per_block = 8 * CAP
-
-    @pl.loop(0, slot_rows // per_block)
-    def _(i):
-        at = pl.ds(pl.multiple_of(i * per_block, per_block), per_block)
-        picked = jnp.dot(slots_v[at, :], normed_v[...], preferred_element_type=F32)
-        out_v[pl.ds(i * 8, 8)] = picked.astype(BF16).reshape(8, CAP, width)
+    def tables(b):
+        @pl.loop(0, 8)
+        def _(i):
+            at = pl.ds(pl.multiple_of(i * 32, 32), 32)
+            x = tok_v[b, at, :].astype(F32)
+            x = x - jnp.mean(x, -1, keepdims=True)
+            var = jnp.mean(x * x, -1, keepdims=True)
+            normed_v[b, at, :] = (x * lax.rsqrt(var + 1e-06) * gain_ref[...]).astype(BF16)
+
+        expert_ids = lax.broadcasted_iota(jnp.int32, (served, tokens), 0) * 2 + parity
+        is_first = expert_ids == routes_ref[b, 0:1, :]
+        is_second = expert_ids == routes_ref[b, 1:2, :]
+        named = is_first | is_second
+        before = (
+            lax.broadcasted_iota(jnp.int32, (tokens, tokens), 0)
+            < lax.broadcasted_iota(jnp.int32, (tokens, tokens), 1)
+        ).astype(F32)
+        rank = jnp.dot(
+            named.astype(F32).astype(BF16), before.astype(BF16), preferred_element_type=F32
+        )
+        rank = jnp.where(named, rank, -1.0)
+        weight = jnp.where(is_first, rw_ref[b, 0:1, :], 0.0) + jnp.where(
+            is_second, rw_ref[b, 1:2, :], 0.0
+        )
+
+        expert, _ = slot_expert((table_rows, served), 0)
+        spread = (
+            expert == lax.broadcasted_iota(jnp.int32, (table_rows, served), 1).astype(F32)
+        ).astype(F32)
+        _, place_t = slot_expert((table_rows, tokens), 0)
+        ranks = jnp.dot(spread.astype(BF16), rank.astype(BF16), preferred_element_type=F32)
+        slots_v[b] = jnp.where(ranks == place_t, 1.0, 0.0).astype(BF16)
+
+        @pl.loop(0, table_rows // per_block)
+        def _(i):
+            at = pl.ds(pl.multiple_of(i * per_block, per_block), per_block)
+            picked = jnp.dot(slots_v[b, at, :], normed_v[b], preferred_element_type=F32)
+            out_v[pl.ds(i * 8, 8), b] = picked.astype(BF16).reshape(8, CAP, width)
+
+        return rank, weight
+
+    def dispatch(b):
+        @pl.loop(0, served)
+        def _(d):
+            expert = lax.rem(place + d * STEP, served)
+            to = expert * 2 + parity
+
+            @pl.when(to != ep)
+            def _():
+                remote(
+                    out_v.at[expert, b], arr_v.at[ep, b], sent_sem.at[11 + b], disp_sem.at[b], (to, tp)
+                ).start()
+
+        @pl.when(at_site)
+        def _():
+            arr_v[ep, b] = out_v[place, b]
+
+    def combine_table(b, rank, weight):
+        expert_c, _ = slot_expert((served, table_rows), 1)
+        spread_t = (
+            expert_c == lax.broadcasted_iota(jnp.int32, (served, table_rows), 0).astype(F32)
+        ).astype(F32).astype(BF16)
+
+        def over_slots(table):
+            return jnp.dot(table.T.astype(BF16), spread_t, preferred_element_type=F32)
+
+        _, place_c = slot_expert((tokens, table_rows), 1)
+        chosen = over_slots(rank) == place_c
+        weight_hi = weight.astype(BF16).astype(F32)
+        comb_v[b, 0] = jnp.where(chosen, over_slots(weight_hi), 0.0).astype(BF16)
+        comb_v[b, 1] = jnp.where(chosen, over_slots(weight - weight_hi), 0.0).astype(BF16)
+
+    loads[0].wait()
+    for k in range(6, 10):
+        loads[k].wait()
+    own_tables = tables(0)
 
     @pl.when(later_count > 0)
     def _():
@@ -300,31 +355,22 @@
 
     for copy in halos:
         copy.start()
-
-    @pl.loop(1, n_ep)
-    def _(d):
-        to = lax.rem(ep + d * STEP, n_ep)
-        remote(out_v.at[to], arr_v.at[ep], disp_sem.at[0], disp_sem.at[1], (to, tp)).start()
-
-    arr_v[ep] = out_v[ep]
-
-    expert_c = jnp.floor((lax.broadcasted_iota(jnp.int32, (n_ep, slot_rows), 1).astype(F32) + 0.5) * (1.0 / CAP))
-    spread_t = (
-        expert_c == lax.broadcasted_iota(jnp.int32, (n_ep, slot_rows), 0).astype(F32)
-    ).astype(F32).astype(BF16)
-
-    def over_slots(table):
-        return lax.dot_general(
-            table.astype(F32).T.astype(BF16),
-            spread_t,
-            (((1,), (0,)), ((), ())),
-            preferred_element_type=F32,
-        )
-
-    _, place_c = slot_expert((tokens, slot_rows), 1)
-    chosen = over_slots(rank) == place_c
-    comb_v[0] = jnp.where(chosen, over_slots(weight_hi), 0.0).astype(BF16)
-    comb_v[1] = jnp.where(chosen, over_slots(weight_lo), 0.0).astype(BF16)
+    dispatch(0)
+
+    for k in range(2):
+        both_ways(gu_own, k)
+
+    @pl.when(off_site)
+    def _():
+        for k in range(2, GU_CHUNKS):
+            both_ways(gu_own, k)
+
+    @pl.when(at_site)
+    def _():
+        for c in range(DOWN_CHUNKS):
+            both_ways(dn_half, c)
+
+    combine_table(0, *own_tables)
 
     loads[1].wait()
     loads[2].wait()
@@ -367,7 +413,17 @@
 
     blocks = rows // block
 
-    @pl.loop(1, blocks - 1)
+    @pl.loop(1, 5)
+    def _(b):
+        attend(b)
+
+    for copy in exchange:
+        copy.wait_recv()
+    partner_tables = tables(1)
+    dispatch(1)
+    combine_table(1, *partner_tables)
+
+    @pl.loop(5, blocks - 1)
     def _(b):
         attend(b)
 
@@ -378,125 +434,143 @@
     def _(i):
         attend(i * (blocks - 1))
 
-    for k in range(2):
-        take(gu_v.at[1, 0], gu_sem.at[k])
-        both_ways(gu_relay, k)
-
-    arrived = arr_v.at[pl.ds(0, n_ep - 1)]
-    pltpu.make_async_copy(arrived, arrived, disp_sem.at[1]).wait()
-
-    slot_blocks = slot_rows // per_block
-
-    def pass_on(c):
-        take(down_v.at[c, pl.ds(hid, 2 * hid), pl.ds(0, COLUMNS[c])], dn_sem.at[c])
-        both_ways(dn_relay, c)
-        if c == 0:
-            both_ways(dn_own, 1)
-        if c + 2 < DOWN_CHUNKS:
-            both_ways(dn_own, c + 2)
-
-    def widen(s):
+    def send_attended():
+        for send in (att_far, att_near):
+            for p in range(ATT_PARTS):
+                both_ways(send, p)
+
+    @pl.when(off_site)
+    def _():
+        for k in range(2):
+            take(gu_v.at[1, 0], gu_sem.at[k])
+            both_ways(gu_relay, k)
+        for c in range(DOWN_CHUNKS):
+            both_ways(dn_own, c)
+            take(down_v.at[c, pl.ds(0, hid), pl.ds(0, COLUMNS[c])], dn_sem.at[c])
+            both_ways(dn_relay, c)
+        send_attended()
+
+    big_block = 16 * CAP
+    slot_blocks = slot_rows // big_block
+
+    def sources(i):
+        return pl.ds(lax.rem(i, 2) * 16, 16)
+
+    def arrived(i):
+        return arr_v[sources(i), i // 2].reshape(big_block, width)
+
+    def rows_of(i):
+        return pl.ds(pl.multiple_of(i * big_block, big_block), big_block)
+
+    def widen(s, first=0, last=slot_blocks):
+        @pl.loop(first, last)
+        def _(i):
+            x = arrived(i)
+            g = jnp.dot(x, gu_v[s, 0], preferred_element_type=F32)
+            u = jnp.dot(x, gu_v[s, 1], preferred_element_type=F32)
+            at = rows_of(i)
+            hid_v[s, at, :] = (g / (1.0 + jnp.exp(-g)) * u).astype(BF16)
+
+    loads[3].wait()
+    loads[4].wait()
+    take(gu_v.at[0, 0], loc_sem.at[10])
+
+    def part_copy(c):
+        return remote(
+            part_v.at[c], got_v.at[c], sent_sem.at[13], part_sem.at[c], (ep, partner)
+        )
+
+    def combine(c):
+        cols = COLUMNS[c]
+
+        @pl.when(at_site)
+        def _():
+            take(ret_v.at[c, pl.ds(0, served - 1)], ret_sem.at[c])
+
+        @pl.when(off_site)
+        def _():
+            take(ret_v.at[c], ret_sem.at[c])
+
+        def share(b):
+            results = ret_v[c, :, b].reshape(table_rows, cols)
+            return jnp.dot(comb_v[b, 0], results, preferred_element_type=F32) + jnp.dot(
+                comb_v[b, 1], results, preferred_element_type=F32
+            )
+
+        part_v[c] = share(1).astype(BF16)
+        part_copy(c).start()
+        sum_v[c] = share(0)
+
+    def finish(c):
+        take(got_v.at[c], part_sem.at[c])
+        exp_ref[:, of_width(c)] = (sum_v[c] + got_v[c].astype(F32)).astype(BF16)
+
+    @pl.when(at_site)
+    def _():
+        for b in range(2):
+            take(arr_v.at[pl.ds(0, n_ep - 1), b], disp_sem.at[b])
+            widen(0, 2 * b, 2 * b + 2)
+        for k in range(GU_CHUNKS):
+            take(gu_v.at[1, 0], gu_sem.at[k])
+
+        @pl.loop(1, 3)
+        def _(s):
+            widen(s)
+
+        take(gu_v.at[3, 0], gur_sem.at[0])
+
         @pl.loop(0, slot_blocks)
         def _(i):
-            x = arr_v[pl.ds(i * 8, 8)].reshape(per_block, width)
-            g = jnp.dot(x, gu_v[s, 0], preferred_element_type=F32)
-            u = jnp.dot(x, gu_v[s, 1], preferred_element_type=F32)
-            at = pl.ds(pl.multiple_of(i * per_block, per_block), per_block)
-            hid_v[s, at, :] = (g / (1.0 + jnp.exp(-g)) * u).astype(BF16)
-
-    loads[3].wait()
-    loads[4].wait()
-    widen(0)
-    for k in range(2, GU_CHUNKS):
-        take(gu_v.at[1, 0], gu_sem.at[k])
-
-    pass_on(0)
-
-    @pl.loop(1, 3)
-    def _(s):
-        widen(s)
-
-    take(gu_v.at[3, 0], gur_sem.at[0])
-
-    @pl.loop(0, slot_blocks)
-    def _(i):
-        x = arr_v[pl.ds(i * 8, 8)].reshape(per_block, width)
-        g = jnp.dot(x, gu_v[3, 0], preferred_element_type=F32)
-        at = pl.ds(pl.multiple_of(i * per_block, per_block), per_block)
-        silu_v[at, :] = g / (1.0 + jnp.exp(-g))
-
-    take(halo_like, halo_sem.at[0])
-    take(gu_v.at[pl.ds(0, 2)], sent_sem.at[0])
-    sent = out_v.at[pl.ds(0, n_ep - 1)]
-    take(sent, disp_sem.at[0])
-    take(gu_v.at[0, 0], loc_sem.at[10])
-    take(gu_v.at[3, 1], gur_sem.at[1])
-
-    @pl.loop(0, slot_blocks)
-    def _(i):
-        x = arr_v[pl.ds(i * 8, 8)].reshape(per_block, width)
-        u = jnp.dot(x, gu_v[3, 1], preferred_element_type=F32)
-        at = pl.ds(pl.multiple_of(i * per_block, per_block), per_block)
-        hid_v[3, at, :] = (silu_v[at, :] * u).astype(BF16)
-
-    take(gu_v.at[0], sent_sem.at[1])
-
-    def combine(c):
-        cols = COLUMNS[c]
-        got = ret_v.at[c, pl.ds(0, n_ep - 1), :, pl.ds(0, cols)]
-        take(got, ret_sem.at[c])
-        results = ret_v[c, :, :, 0:cols].reshape(slot_rows, cols)
-        total = jnp.dot(comb_v[0], results, preferred_element_type=F32) + jnp.dot(
-            comb_v[1], results, preferred_element_type=F32
-        )
-        exp_ref[:, of_width(c)] = total.astype(BF16)
-
-    for c in range(DOWN_CHUNKS):
-        if 0 < c < DOWN_CHUNKS - 1:
-            pass_on(c + 1)
-        take(down_v.at[c, pl.ds(3 * hid, hid), pl.ds(0, COLUMNS[c])], dnr_sem.at[c])
-
-        cols = COLUMNS[c]
-        span_cols = pl.ds(0, cols)
-
-        @pl.loop(0, slot_rows // per_block)
+            g = jnp.dot(arrived(i), gu_v[3, 0], preferred_element_type=F32)
+            at = rows_of(i)
+            silu_v[at, :] = g / (1.0 + jnp.exp(-g))
+
+        take(gu_v.at[3, 1], gur_sem.at[1])
+
+        @pl.loop(0, slot_blocks)
         def _(i):
-            at = pl.ds(pl.multiple_of(i * per_block, per_block), per_block)
-            total = jnp.zeros((per_block, cols), F32)
-            for s in range(4):
-                total = total + jnp.dot(
-                    hid_v[s, at, :],
-                    down_v[c, s * hid : (s + 1) * hid, 0:cols],
-                    preferred_element_type=F32,
-                )
-            back_v[c, pl.ds(i * 8, 8), :, 0:cols] = total.astype(BF16).reshape(8, CAP, cols)
-
-        @pl.loop(1, n_ep)
-        def _(d):
-            to = lax.rem(ep + d * STEP, n_ep)
-            remote(
-                back_v.at[c, to, :, span_cols],
-                ret_v.at[c, ep, :, span_cols],
-                sent_sem.at[7],
-                ret_sem.at[c],
-                (to, tp),
-            ).start()
-
-        ret_v[c, ep, :, 0:cols] = back_v[c, ep, :, 0:cols]
-        if c == 0:
-            pass_on(1)
-        if c == DOWN_CHUNKS - 2:
-            for send in (att_far, att_near):
-                for p in range(ATT_PARTS):
-                    both_ways(send, p)
-        if 4 <= c < DOWN_CHUNKS - 1:
-            combine(c - 4)
+            u = jnp.dot(arrived(i), gu_v[3, 1], preferred_element_type=F32)
+            at = rows_of(i)
+            hid_v[3, at, :] = (silu_v[at, :] * u).astype(BF16)
+
+        for c in range(DOWN_CHUNKS):
+            cols = COLUMNS[c]
+            take(down_v.at[c, pl.ds(hid, 2 * hid), pl.ds(0, cols)], dn_sem.at[c])
+            take(down_v.at[c, pl.ds(3 * hid, hid), pl.ds(0, cols)], dnr_sem.at[c])
+
+            @pl.loop(0, slot_blocks)
+            def _(i):
+                at = rows_of(i)
+                total = jnp.zeros((big_block, cols), F32)
+                for s in range(4):
+                    total = total + jnp.dot(
+                        hid_v[s, at, :],
+                        down_v[c, s * hid : (s + 1) * hid, 0:cols],
+                        preferred_element_type=F32,
+                    )
+                back_v[c, sources(i), i // 2] = total.astype(BF16).reshape(16, CAP, cols)
+
+            @pl.loop(1, n_ep)
+            def _(d):
+                to = lax.rem(ep + d * STEP, n_ep)
+                remote(
+                    back_v.at[c, to], ret_v.at[c, place], sent_sem.at[7], ret_sem.at[c], (to, tp)
+                ).start()
+
+            ret_v[c, place] = back_v[c, ep]
+            if c == 4:
+                send_attended()
+            if c >= 5:
+                combine(c - 5)
+
+    @pl.when(off_site)
+    def _():
+        for c in range(3):
+            combine(c)
 
     for p in range(ATT_PARTS):
         take(pass_v.at[:, p], far_sem.at[p])
         both_ways(att_fwd, p)
-    take(gu_v.at[0], sent_sem.at[2])
-    take(gu_v.at[0, 0], sent_sem.at[3])
 
     loads[5].wait()
     head_cols = heads * HEAD_DIM
@@ -526,20 +600,48 @@
         take(attin_v.at[opposite, pl.ds(p * part_rows, part_rows)], fwd_sem.at[p])
         add_heads(p, ((opposite, attin_v.at[opposite]),), False)
 
-    combine(DOWN_CHUNKS - 5)
+    combine(3)
+    combine(4)
     project_near(0)
-    combine(DOWN_CHUNKS - 4)
+    combine(5)
     project_near(1)
-    combine(DOWN_CHUNKS - 3)
+    for c in range(4):
+        finish(c)
+    combine(6)
     for p in range(ATT_PARTS):
         project_far(p)
-    combine(DOWN_CHUNKS - 2)
+    for c in range(4, 6):
+        finish(c)
+    combine(7)
+
+    take(kv_v.at[pl.ds(0, 2 * WINDOW)], halo_sem.at[0])
+    for copy in exchange:
+        copy.wait_send()
+
+    @pl.when(at_site)
+    def _():
+        take(gu_v.at[0], sent_sem.at[0])
+        take(gu_v.at[0, 0], sent_sem.at[2])
+        for b in range(2):
+            take(out_v.at[pl.ds(0, served - 1), b], sent_sem.at[11 + b])
+        for c in range(DOWN_CHUNKS):
+            take(back_v.at[c, pl.ds(0, n_ep - 1)], sent_sem.at[7])
+
+    @pl.when(off_site)
+    def _():
+        take(gu_v.at[pl.ds(0, 2)], sent_sem.at[0])
+        take(gu_v.at[0], sent_sem.at[1])
+        take(gu_v.at[0], sent_sem.at[2])
+        take(gu_v.at[0, 0], sent_sem.at[3])
+        for b in range(2):
+            take(out_v.at[:, b], sent_sem.at[11 + b])
 
     take(attin_v.at[0], sent_sem.at[4])
     take(attin_v.at[0], sent_sem.at[5])
     take(attin_v.at[pl.ds(0, 2)], sent_sem.at[6])
-    combine(DOWN_CHUNKS - 1)
-    take(sent, sent_sem.at[7])
+    finish(6)
+    finish(7)
+    take(part_v, sent_sem.at[13])
 
 
 def put_out(mix_ref, exp_ref, mix_hbm, exp_hbm, sem):
@@ -573,7 +675,9 @@
     hid = gate_weight.shape[2]
     out_rows = rows // n_tp
     dcol = max(COLUMNS)
-    slot_rows = n_ep * CAP
+    served = n_ep // 2
+    slot_rows = 2 * n_ep * CAP
+    table_rows = served * CAP
     hbm = pl.BlockSpec(memory_space=pltpu.HBM)
     vmem = pl.BlockSpec(memory_space=pltpu.VMEM)
     dma = pltpu.SemaphoreType.DMA
@@ -588,31 +692,34 @@
         scratch_shapes=[
             pltpu.SMEM(sink_logits.shape, F32),
             pltpu.VMEM((1, width), F32),
-            pltpu.VMEM((2, tokens), jnp.int32),
-            pltpu.VMEM((2, tokens), F32),
+            pltpu.VMEM((2, 2, tokens), jnp.int32),
+            pltpu.VMEM((2, 2, tokens), F32),
             pltpu.VMEM((rows, q_cols), BF16),
             pltpu.VMEM((rows + 2 * WINDOW, 2 * HEAD_DIM), BF16),
             pltpu.VMEM(out_weight.shape, BF16),
-            pltpu.VMEM((tokens, width), BF16),
-            pltpu.VMEM((tokens, width), BF16),
-            pltpu.VMEM((slot_rows, tokens), BF16),
-            pltpu.VMEM((2, tokens, slot_rows), BF16),
-            pltpu.VMEM((n_ep, CAP, width), BF16),
-            pltpu.VMEM((n_ep, CAP, width), BF16),
+            pltpu.VMEM((2, tokens, width), BF16),
+            pltpu.VMEM((2, tokens, width), BF16),
+            pltpu.VMEM((2, table_rows, tokens), BF16),
+            pltpu.VMEM((2, 2, tokens, table_rows), BF16),
+            pltpu.VMEM((served, 2, CAP, width), BF16),
+            pltpu.VMEM((n_ep, 2, CAP, width), BF16),
             pltpu.VMEM((4, 2, width, hid), BF16),
             pltpu.VMEM((DOWN_CHUNKS, 4 * hid, dcol), BF16),
             pltpu.VMEM((4, slot_rows, hid), BF16),
-            pltpu.VMEM((DOWN_CHUNKS, n_ep, CAP, dcol), BF16),
-            pltpu.VMEM((DOWN_CHUNKS, n_ep, CAP, dcol), BF16),
+            pltpu.VMEM((DOWN_CHUNKS, n_ep, 2, CAP, dcol), BF16),
+            pltpu.VMEM((DOWN_CHUNKS, served, 2, CAP, dcol), BF16),
             pltpu.VMEM((n_tp, out_rows, q_cols), BF16),
             pltpu.VMEM((n_tp, out_rows, q_cols), BF16),
             pltpu.VMEM((2, ATT_PARTS, out_rows // ATT_PARTS, q_cols // 2), BF16),
             pltpu.VMEM((out_rows, width), F32),
             pltpu.VMEM((slot_rows, hid), F32),
+            pltpu.VMEM((DOWN_CHUNKS, tokens, dcol), BF16),
+            pltpu.VMEM((DOWN_CHUNKS, tokens, dcol), F32),
+            pltpu.VMEM((DOWN_CHUNKS, tokens, dcol), BF16),
             pltpu.SemaphoreType.REGULAR,
             dma((11,)),
             dma((2,)),
-            dma((8,)),
+            dma((14,)),
             dma((GU_CHUNKS,)),
             dma((2,)),
             dma((DOWN_CHUNKS,)),
@@ -622,9 +729,11 @@
             dma((ATT_PARTS,)),
             dma((ATT_PARTS,)),
             dma((ATT_PARTS,)),
+            dma((3,)),
+            dma((DOWN_CHUNKS,)),
         ],
         compiler_params=pltpu.CompilerParams(
-            collective_id=0, has_side_effects=True, vmem_limit_bytes=52 * 1024 * 1024
+            collective_id=0, has_side_effects=True, vmem_limit_bytes=59 * 1024 * 1024
         ),
     )(
         *(

time: 126 us -> 121 us (0.960)
  Pallas kernels: 125 us -> 119 us
    pallas_call x1, Pallas kernels: 123 us -> 117 us  [body(): pl.pallas_call(functools.partial(kernel, n_ep, n_tp), out_shape=(pltpu.VM...]
where the time goes in v5:
time: 121 us; the launch traced here: 120 us
  Pallas kernels  119 us (98%)
    pallas_call x1, Pallas kernels, body(): pl.pallas_call(functools.partial(kernel, n_ep, n_tp), out_shape=(pltpu.VM...  117 us

profile of v5, /device:TPU:0, one launch (start us, length us, event | category | flops | bytes accessed | tf_op | source)
XLA Modules:
  0.0 119.7 jit_solution(8542487030577737775)
XLA Ops:
  0.6 117.2 %shard_map.122 = (bf16[512,2048]{1,0:T(8,128)(2,1)S(1)}, bf16[256,2048]{1,0:T(8,128)(2,1)S(1)}) custom-call(bf16[2048,256]{1,0:T(8,128)(2,1)} %q_hbm.1, bf16[2048,128]{1,0:T(8,128)(2,1)} %kv_hbm.1, f32[16]{0:T(128)} %sink_hbm.1, bf16[1024,2048]{1,0:T(8,128)(2,1)} %ow_hbm.1, bf16[256,2048]{1,0:T(8,128)(2,1)} %tok_hbm.1, f32[1,2048]{1,0:T(1,128)} %bitcast.3, ...), custom_call_target="tpu_custom_call" | custom-call | tf_op jit(solution)/shard_map/pallas_call | solution.py:684
  117.9 1.7 %shard_map.123 = (bf16[512,2048]{1,0:T(8,128)(2,1)}, bf16[256,2048]{1,0:T(8,128)(2,1)}) custom-call(bf16[512,2048]{1,0:T(8,128)(2,1)S(1)} %get-tuple-element.4.mix_ref, bf16[256,2048]{1,0:T(8,128)(2,1)S(1)} %get-tuple-element.5.exp_ref), custom_call_target="tpu_custom_call" | custom-call | tf_op jit(solution)/shard_map/pallas_call | solution.py:756

commit v6 on v5

--- a/solution.py
+++ b/solution.py
@@ -12,7 +12,7 @@
 WINDOW = 128
 CAP = 24
 SIDE = 4
-STEP = 13
+STEP = 7
 F32 = jnp.float32
 BF16 = jnp.bfloat16
 NEG_FILL = -1e30
@@ -21,6 +21,7 @@
 COLUMNS = (256,) * 8
 DOWN_CHUNKS = len(COLUMNS)
 ATT_PARTS = 2
+EARLY = 2
 
 
 def kernel(
@@ -357,19 +358,6 @@
         copy.start()
     dispatch(0)
 
-    for k in range(2):
-        both_ways(gu_own, k)
-
-    @pl.when(off_site)
-    def _():
-        for k in range(2, GU_CHUNKS):
-            both_ways(gu_own, k)
-
-    @pl.when(at_site)
-    def _():
-        for c in range(DOWN_CHUNKS):
-            both_ways(dn_half, c)
-
     combine_table(0, *own_tables)
 
     loads[1].wait()
@@ -413,17 +401,31 @@
 
     blocks = rows // block
 
-    @pl.loop(1, 5)
+    @pl.loop(1, 3)
     def _(b):
         attend(b)
 
+    for k in range(2):
+        both_ways(gu_own, k)
+
+    @pl.when(off_site)
+    def _():
+        for k in range(2, GU_CHUNKS):
+            both_ways(gu_own, k)
+
+    @pl.when(at_site)
+    def _():
+        for c in range(EARLY):
+            both_ways(dn_half, c)
+
+    attend(3)
     for copy in exchange:
         copy.wait_recv()
     partner_tables = tables(1)
     dispatch(1)
     combine_table(1, *partner_tables)
 
-    @pl.loop(5, blocks - 1)
+    @pl.loop(4, blocks - 1)
     def _(b):
         attend(b)
 
@@ -516,6 +518,9 @@
         @pl.loop(1, 3)
         def _(s):
             widen(s)
+
+        for c in range(EARLY, DOWN_CHUNKS):
+            both_ways(dn_half, c)
 
         take(gu_v.at[3, 0], gur_sem.at[0])
 

time: 121 us -> 119 us (0.983)
  Pallas kernels: 119 us -> 117 us
    pallas_call x1, Pallas kernels: 117 us -> 115 us  [body(): pl.pallas_call(functools.partial(kernel, n_ep, n_tp), out_shape=(pltpu.VM...]
where the time goes in v6:
time: 119 us; the launch traced here: 118 us
  Pallas kernels  117 us (98%)
    pallas_call x1, Pallas kernels, body(): pl.pallas_call(functools.partial(kernel, n_ep, n_tp), out_shape=(pltpu.VM...  115 us

profile of v6, /device:TPU:0, one launch (start us, length us, event | category | flops | bytes accessed | tf_op | source)
XLA Modules:
  0.0 117.9 jit_solution(1401871842312174864)
XLA Ops:
  0.6 115.4 %shard_map.122 = (bf16[512,2048]{1,0:T(8,128)(2,1)S(1)}, bf16[256,2048]{1,0:T(8,128)(2,1)S(1)}) custom-call(bf16[2048,256]{1,0:T(8,128)(2,1)} %q_hbm.1, bf16[2048,128]{1,0:T(8,128)(2,1)} %kv_hbm.1, f32[16]{0:T(128)} %sink_hbm.1, bf16[1024,2048]{1,0:T(8,128)(2,1)} %ow_hbm.1, bf16[256,2048]{1,0:T(8,128)(2,1)} %tok_hbm.1, f32[1,2048]{1,0:T(1,128)} %bitcast.3, ...), custom_call_target="tpu_custom_call" | custom-call | tf_op jit(solution)/shard_map/pallas_call | solution.py:689
  116.0 1.7 %shard_map.123 = (bf16[512,2048]{1,0:T(8,128)(2,1)}, bf16[256,2048]{1,0:T(8,128)(2,1)}) custom-call(bf16[512,2048]{1,0:T(8,128)(2,1)S(1)} %get-tuple-element.4.mix_ref, bf16[256,2048]{1,0:T(8,128)(2,1)S(1)} %get-tuple-element.5.exp_ref), custom_call_target="tpu_custom_call" | custom-call | tf_op jit(solution)/shard_map/pallas_call | solution.py:761

commit v7 on v6

--- a/solution.py
+++ b/solution.py
@@ -18,10 +18,10 @@
 NEG_FILL = -1e30
 
 GU_CHUNKS = 4
-COLUMNS = (256,) * 8
+COLUMNS = (128,) + (256,) * 7 + (128,)
 DOWN_CHUNKS = len(COLUMNS)
 ATT_PARTS = 2
-EARLY = 2
+EARLY = 1
 
 
 def kernel(
@@ -62,7 +62,6 @@
     attin_v,
     pass_v,
     acc_v,
-    silu_v,
     part_v,
     sum_v,
     got_v,
@@ -461,6 +460,9 @@
     def arrived(i):
         return arr_v[sources(i), i // 2].reshape(big_block, width)
 
+    def silu_cols(i):
+        return pl.ds(pl.multiple_of(i * hid, hid), hid)
+
     def rows_of(i):
         return pl.ds(pl.multiple_of(i * big_block, big_block), big_block)
 
@@ -478,8 +480,9 @@
     take(gu_v.at[0, 0], loc_sem.at[10])
 
     def part_copy(c):
+        at = pl.ds(0, COLUMNS[c])
         return remote(
-            part_v.at[c], got_v.at[c], sent_sem.at[13], part_sem.at[c], (ep, partner)
+            part_v.at[c, :, at], got_v.at[c, :, at], sent_sem.at[13], part_sem.at[c], (ep, partner)
         )
 
     def combine(c):
@@ -487,25 +490,26 @@
 
         @pl.when(at_site)
         def _():
-            take(ret_v.at[c, pl.ds(0, served - 1)], ret_sem.at[c])
+            take(ret_v.at[c, pl.ds(0, served - 1), :, :, pl.ds(0, cols)], ret_sem.at[c])
 
         @pl.when(off_site)
         def _():
-            take(ret_v.at[c], ret_sem.at[c])
+            take(ret_v.at[c, :, :, :, pl.ds(0, cols)], ret_sem.at[c])
 
         def share(b):
-            results = ret_v[c, :, b].reshape(table_rows, cols)
+            results = ret_v[c, :, b, :, 0:cols].reshape(table_rows, cols)
             return jnp.dot(comb_v[b, 0], results, preferred_element_type=F32) + jnp.dot(
                 comb_v[b, 1], results, preferred_element_type=F32
             )
 
-        part_v[c] = share(1).astype(BF16)
+        part_v[c, :, 0:cols] = share(1).astype(BF16)
         part_copy(c).start()
-        sum_v[c] = share(0)
+        sum_v[c, :, 0:cols] = share(0)
 
     def finish(c):
-        take(got_v.at[c], part_sem.at[c])
-        exp_ref[:, of_width(c)] = (sum_v[c] + got_v[c].astype(F32)).astype(BF16)
+        cols = COLUMNS[c]
+        take(got_v.at[c, :, pl.ds(0, cols)], part_sem.at[c])
+        exp_ref[:, of_width(c)] = (sum_v[c, :, 0:cols] + got_v[c, :, 0:cols].astype(F32)).astype(BF16)
 
     @pl.when(at_site)
     def _():
@@ -527,8 +531,7 @@
         @pl.loop(0, slot_blocks)
         def _(i):
             g = jnp.dot(arrived(i), gu_v[3, 0], preferred_element_type=F32)
-            at = rows_of(i)
-            silu_v[at, :] = g / (1.0 + jnp.exp(-g))
+            acc_v[0:big_block, silu_cols(i)] = g / (1.0 + jnp.exp(-g))
 
         take(gu_v.at[3, 1], gur_sem.at[1])
 
@@ -536,7 +539,7 @@
         def _(i):
             u = jnp.dot(arrived(i), gu_v[3, 1], preferred_element_type=F32)
             at = rows_of(i)
-            hid_v[3, at, :] = (silu_v[at, :] * u).astype(BF16)
+            hid_v[3, at, :] = (acc_v[0:big_block, silu_cols(i)] * u).astype(BF16)
 
         for c in range(DOWN_CHUNKS):
             cols = COLUMNS[c]
@@ -553,16 +556,20 @@
                         down_v[c, s * hid : (s + 1) * hid, 0:cols],
                         preferred_element_type=F32,
                     )
-                back_v[c, sources(i), i // 2] = total.astype(BF16).reshape(16, CAP, cols)
+                back_v[c, sources(i), i // 2, :, 0:cols] = total.astype(BF16).reshape(16, CAP, cols)
 
             @pl.loop(1, n_ep)
             def _(d):
                 to = lax.rem(ep + d * STEP, n_ep)
                 remote(
-                    back_v.at[c, to], ret_v.at[c, place], sent_sem.at[7], ret_sem.at[c], (to, tp)
+                    back_v.at[c, to, :, :, pl.ds(0, cols)],
+                    ret_v.at[c, place, :, :, pl.ds(0, cols)],
+                    sent_sem.at[7],
+                    ret_sem.at[c],
+                    (to, tp),
                 ).start()
 
-            ret_v[c, place] = back_v[c, ep]
+            ret_v[c, place, :, :, 0:cols] = back_v[c, ep, :, :, 0:cols]
             if c == 4:
                 send_attended()
             if c >= 5:
@@ -570,7 +577,7 @@
 
     @pl.when(off_site)
     def _():
-        for c in range(3):
+        for c in range(4):
             combine(c)
 
     for p in range(ATT_PARTS):
@@ -605,19 +612,19 @@
         take(attin_v.at[opposite, pl.ds(p * part_rows, part_rows)], fwd_sem.at[p])
         add_heads(p, ((opposite, attin_v.at[opposite]),), False)
 
-    combine(3)
     combine(4)
+    combine(5)
     project_near(0)
-    combine(5)
+    combine(6)
     project_near(1)
-    for c in range(4):
+    for c in range(5):
         finish(c)
-    combine(6)
+    combine(7)
     for p in range(ATT_PARTS):
         project_far(p)
-    for c in range(4, 6):
+    for c in range(5, 7):
         finish(c)
-    combine(7)
+    combine(8)
 
     take(kv_v.at[pl.ds(0, 2 * WINDOW)], halo_sem.at[0])
     for copy in exchange:
@@ -630,7 +637,7 @@
         for b in range(2):
             take(out_v.at[pl.ds(0, served - 1), b], sent_sem.at[11 + b])
         for c in range(DOWN_CHUNKS):
-            take(back_v.at[c, pl.ds(0, n_ep - 1)], sent_sem.at[7])
+            take(back_v.at[c, pl.ds(0, n_ep - 1), :, :, pl.ds(0, COLUMNS[c])], sent_sem.at[7])
 
     @pl.when(off_site)
     def _():
@@ -644,9 +651,9 @@
     take(attin_v.at[0], sent_sem.at[4])
     take(attin_v.at[0], sent_sem.at[5])
     take(attin_v.at[pl.ds(0, 2)], sent_sem.at[6])
-    finish(6)
     finish(7)
-    take(part_v, sent_sem.at[13])
+    finish(8)
+    take(normed_v.at[0], sent_sem.at[13])
 
 
 def put_out(mix_ref, exp_ref, mix_hbm, exp_hbm, sem):
@@ -717,7 +724,6 @@
             pltpu.VMEM((n_tp, out_rows, q_cols), BF16),
             pltpu.VMEM((2, ATT_PARTS, out_rows // ATT_PARTS, q_cols // 2), BF16),
             pltpu.VMEM((out_rows, width), F32),
-            pltpu.VMEM((slot_rows, hid), F32),
             pltpu.VMEM((DOWN_CHUNKS, tokens, dcol), BF16),
             pltpu.VMEM((DOWN_CHUNKS, tokens, dcol), F32),
             pltpu.VMEM((DOWN_CHUNKS, tokens, dcol), BF16),
@@ -738,7 +744,7 @@
             dma((DOWN_CHUNKS,)),
         ],
         compiler_params=pltpu.CompilerParams(
-            collective_id=0, has_side_effects=True, vmem_limit_bytes=59 * 1024 * 1024
+            collective_id=0, has_side_effects=True, vmem_limit_bytes=60 * 1024 * 1024
         ),
     )(
         *(

time: 119 us -> 117 us (0.983)
    pallas_call x1, Pallas kernels: 115 us -> 114 us  [body(): pl.pallas_call(functools.partial(kernel, n_ep, n_tp), out_shape=(pltpu.VM...]
where the time goes in v7:
time: 117 us; the launch traced here: 116 us
  Pallas kernels  116 us (99%)
    pallas_call x1, Pallas kernels, body(): pl.pallas_call(functools.partial(kernel, n_ep, n_tp), out_shape=(pltpu.VM...  114 us

profile of v7, /device:TPU:0, one launch (start us, length us, event | category | flops | bytes accessed | tf_op | source)
XLA Modules:
  0.0 116.4 jit_solution(6071813678205893941)
XLA Ops:
  0.6 113.9 %shard_map.122 = (bf16[512,2048]{1,0:T(8,128)(2,1)S(1)}, bf16[256,2048]{1,0:T(8,128)(2,1)S(1)}) custom-call(bf16[2048,256]{1,0:T(8,128)(2,1)} %q_hbm.1, bf16[2048,128]{1,0:T(8,128)(2,1)} %kv_hbm.1, f32[16]{0:T(128)} %sink_hbm.1, bf16[1024,2048]{1,0:T(8,128)(2,1)} %ow_hbm.1, bf16[256,2048]{1,0:T(8,128)(2,1)} %tok_hbm.1, f32[1,2048]{1,0:T(1,128)} %bitcast.3, ...), custom_call_target="tpu_custom_call" | custom-call | tf_op jit(solution)/shard_map/pallas_call | solution.py:696
  114.5 1.7 %shard_map.123 = (bf16[512,2048]{1,0:T(8,128)(2,1)}, bf16[256,2048]{1,0:T(8,128)(2,1)}) custom-call(bf16[512,2048]{1,0:T(8,128)(2,1)S(1)} %get-tuple-element.4.mix_ref, bf16[256,2048]{1,0:T(8,128)(2,1)S(1)} %get-tuple-element.5.exp_ref), custom_call_target="tpu_custom_call" | custom-call | tf_op jit(solution)/shard_map/pallas_call | solution.py:767
